TPU v7x, 32 devices: a whole 2x2x4 slice. The times are simulated.
32 devices in a mesh: sp: 8 (over z, x), tp: 4 (over y, core).
Axes of the slice: x: 2, y: 2, z: 4, core: 2. Of those that a mesh axis runs over, the one named last changes fastest.
Arguments:
- residual_in: bfloat16 [1024, 2048], P('sp', 'tp'), may hold values from -8 to 8
- query_alpha: bfloat16 [1024, 2048], P('sp', 'tp'), may hold values from -8 to 8
- pairs_alpha: bfloat16 [1024, 16, 128], P('sp', 'tp'), may hold values from -8 to 8
- offset_alpha: float32 [1024, 32], P('sp', 'tp'), may hold values from -18 to -1
- gain_alpha: float32 [2048], P('tp'), may hold values from 0.1 to 1.9
- query_beta: bfloat16 [1024, 2048], P('sp', 'tp'), may hold values from -8 to 8
- pairs_beta: bfloat16 [1024, 16, 256], P('sp', 'tp'), may hold values from -8 to 8
- offset_beta: float32 [1024, 16], P('sp', 'tp'), may hold values from -18 to -1
- gain_beta: float32 [2048], P('tp'), may hold values from 0.1 to 1.9
- project_alpha: bfloat16 [2048, 2048], P('tp'), may hold values from -0.09375 to 0.09375
- project_beta: bfloat16 [2048, 2048], P('tp'), may hold values from -0.09375 to 0.09375
- gain_settle: float32 [2048], P('tp'), may hold values from 0 to 4
- bias_settle: float32 [2048], P('tp'), may hold values from -2.5 to 2.5
- expert_ids: int32 [1024, 2], P('sp'), may hold values from 0 to 7, as said below
- route_weight: float32 [1024, 2], P('sp'), may hold values from 0.1 to 0.9
- expert_gate: bfloat16 [8, 2048, 4096], P('sp', None, 'tp'), may hold values from -0.125 to 0.125
- expert_up: bfloat16 [8, 2048, 4096], P('sp', None, 'tp'), may hold values from -0.125 to 0.125
- expert_down: bfloat16 [8, 4096, 2048], P('sp', 'tp'), may hold values from -0.1875 to 0.1875
- gain_final: float32 [2048], P('tp'), may hold values from 0.1 to 1.9
- bias_final: float32 [2048], P('tp'), may hold values from -2.5 to 2.5
Outputs:
- layer_out: bfloat16 [1024, 2048], P('sp', 'tp')
Inputs may be any that keep to these rules, and one draw needn't show every extreme that they name: `expert_ids`: the two numbers of a row differ and lie in one group of 2 consecutive experts. Among the rows of one device, no expert is named more than 48 times, and every expert of one group, the same group for all devices, is named exactly 48 times.
All inputs are finite; a program needn't handle non-finite values.
Results may differ from a plain program's by a relative error of at most 0.018.
Values may be sent and summed in bfloat16 or wider, within the bound.
No kernel may reach another device: no remote copies, remote signals or barrier semaphores. Data moves between devices by JAX's collectives and lax.ppermute only.
A program may use at most 64 MiB of HBM per device.

v0:
```python
import jax
import jax.numpy as jnp
from jax import lax
from jax.experimental import pallas as pl
from jax.experimental.pallas import tpu as pltpu
from jax.sharding import PartitionSpec as P


depth_scale = 2.0**0.5
norm_eps = 1e-05


def break_block(acc, remain, queries, pairs, offsets, key_first, query_first):
    width = queries.shape[3]
    keys = pairs[:, :, :width]
    values = pairs[:, :, width:]
    length = offsets.shape[0]
    kv_heads = queries.shape[1]
    share = queries.shape[2]
    scores = jnp.einsum(
        "qhrd,khd->hrqk", queries, keys, preferred_element_type=jnp.float32
    ) * width ** (-0.5)
    scores = (
        scores + jnp.transpose(offsets.reshape(length, kv_heads, share), (1, 2, 0))[:, :, None, :]
    )
    query_pos = query_first + jnp.arange(queries.shape[0], dtype=jnp.int32)
    key_pos = key_first + jnp.arange(length, dtype=jnp.int32)
    valid = key_pos[None, :] < query_pos[:, None]
    soft = jnp.where(valid, jax.nn.softplus(scores), 0.0)
    later = lax.cumsum(soft, axis=3, reverse=True) - soft
    weights = jnp.where(
        valid, jnp.exp(jax.nn.log_sigmoid(scores) - later + remain[..., None]), 0.0
    ).astype(jnp.bfloat16)
    acc = acc + jnp.einsum("hrqk,khd->qhrd", weights, values, preferred_element_type=jnp.float32)
    return (acc, remain - jnp.sum(soft, axis=3))


def finish_norm(total, sums, gain, bias, columns):
    mean = sums[0] / columns
    var = sums[1] / columns - mean * mean
    return ((total - mean[:, None]) * lax.rsqrt(var + norm_eps)[:, None] * gain + bias).astype(
        jnp.bfloat16
    )


def general_body(
    residual_in,
    query_alpha,
    pairs_alpha,
    offset_alpha,
    gain_alpha,
    query_beta,
    pairs_beta,
    offset_beta,
    gain_beta,
    project_alpha,
    project_beta,
    gain_settle,
    bias_settle,
    expert_ids,
    route_weight,
    expert_gate,
    expert_up,
    expert_down,
    gain_final,
    bias_final,
):
    rows = residual_in.shape[0]
    mine = lax.axis_index("sp")
    count = lax.axis_size("sp")
    heads_tp = lax.axis_size("tp")
    width_alpha = pairs_alpha.shape[2] // 2
    width_beta = pairs_beta.shape[2] // 2
    grouped_alpha = query_alpha.reshape(rows, pairs_alpha.shape[1], -1, width_alpha)
    grouped_beta = query_beta.reshape(rows, pairs_beta.shape[1], -1, width_beta)
    query_first = mine * rows
    initial = (
        jnp.zeros(grouped_alpha.shape, jnp.float32),
        jnp.zeros(grouped_beta.shape, jnp.float32),
        jnp.zeros((grouped_alpha.shape[1], grouped_alpha.shape[2], rows), jnp.float32),
        jnp.zeros((grouped_beta.shape[1], grouped_beta.shape[2], rows), jnp.float32),
    )

    def visit(state, pairs, offsets, key_first):
        acc_alpha, acc_beta, rest_alpha, rest_beta = state
        acc_alpha, rest_alpha = break_block(
            acc_alpha, rest_alpha, grouped_alpha, pairs[0], offsets[0], key_first, query_first
        )
        acc_beta, rest_beta = break_block(
            acc_beta, rest_beta, grouped_beta, pairs[1], offsets[1], key_first, query_first
        )
        return (acc_alpha, acc_beta, rest_alpha, rest_beta)

    def maybe_visit(state, turn, pairs, offsets):
        return lax.cond(
            turn <= mine,
            lambda kept: visit(kept, pairs, offsets, (mine - turn) * rows),
            lambda kept: kept,
            state,
        )

    pairs_all = (
        lax.all_gather(pairs_alpha, "sp", axis=0, tiled=True),
        lax.all_gather(pairs_beta, "sp", axis=0, tiled=True),
    )
    offsets_all = (
        lax.all_gather(offset_alpha, "sp", axis=0, tiled=True),
        lax.all_gather(offset_beta, "sp", axis=0, tiled=True),
    )

    def turn_all(turn, state):
        first_row = (mine - turn) * rows
        pairs = (
            lax.dynamic_slice_in_dim(pairs_all[0], first_row, rows, 0),
            lax.dynamic_slice_in_dim(pairs_all[1], first_row, rows, 0),
        )
        offsets = (
            lax.dynamic_slice_in_dim(offsets_all[0], first_row, rows, 0),
            lax.dynamic_slice_in_dim(offsets_all[1], first_row, rows, 0),
        )
        return maybe_visit(state, turn, pairs, offsets)

    state = lax.fori_loop(0, count, turn_all, initial)
    attend_alpha = state[0].reshape(rows, -1)
    attend_beta = state[1].reshape(rows, -1)
    squares = lax.psum(
        (jnp.sum(attend_alpha * attend_alpha, axis=1), jnp.sum(attend_beta * attend_beta, axis=1)),
        "tp",
    )
    scale_alpha = lax.rsqrt(squares[0] / (attend_alpha.shape[1] * heads_tp) + norm_eps)
    scale_beta = lax.rsqrt(squares[1] / (attend_beta.shape[1] * heads_tp) + norm_eps)
    normed_alpha = (attend_alpha * scale_alpha[:, None] * gain_alpha).astype(jnp.bfloat16)
    normed_beta = (attend_beta * scale_beta[:, None] * gain_beta).astype(jnp.bfloat16)
    term = jnp.dot(normed_alpha, project_alpha, preferred_element_type=jnp.float32) + jnp.dot(
        normed_beta, project_beta, preferred_element_type=jnp.float32
    )
    mixed = lax.psum_scatter(term.astype(jnp.bfloat16), "tp", scatter_dimension=1, tiled=True)
    columns = residual_in.shape[1] * heads_tp
    first = depth_scale * residual_in.astype(jnp.float32) + mixed.astype(jnp.float32)
    sums_one = lax.psum((jnp.sum(first, axis=1), jnp.sum(first * first, axis=1)), "tp")
    settled = finish_norm(first, sums_one, gain_settle, bias_settle, columns)
    cap = 3 * rows // count
    flat_ids = expert_ids.reshape(2 * rows)
    onehot = (flat_ids[:, None] == jnp.arange(count, dtype=jnp.int32)[None, :]).astype(jnp.int32)
    before = jnp.cumsum(onehot, axis=0, dtype=jnp.int32) - onehot
    slot = jnp.sum(before * onehot, axis=1, dtype=jnp.int32)
    place = flat_ids * cap + slot
    hit = place[None, :] == jnp.arange(count * cap, dtype=jnp.int32)[:, None]
    owner = jnp.arange(2 * rows, dtype=jnp.int32) // 2
    source = jnp.sum(jnp.where(hit, owner[None, :], 0), axis=1, dtype=jnp.int32)
    filled = jnp.any(hit, axis=1)
    gate_local = expert_gate[0]
    up_local = expert_up[0]
    send = jnp.where(filled[:, None], settled[source], jnp.zeros((), jnp.bfloat16)).reshape(
        count, cap, -1
    )
    arrived = lax.all_to_all(send, "sp", split_axis=0, concat_axis=0, tiled=True)
    piece = lax.all_gather(arrived, "tp", axis=2, tiled=True)
    flat = piece.reshape(-1, piece.shape[2])
    gate = jnp.dot(flat, gate_local, preferred_element_type=jnp.float32)
    up = jnp.dot(flat, up_local, preferred_element_type=jnp.float32)
    hidden = (jax.nn.silu(gate) * up).astype(jnp.bfloat16)
    partial_value = jnp.dot(hidden, expert_down[0], preferred_element_type=jnp.float32).reshape(
        count, cap, -1
    )
    summed = lax.psum_scatter(
        partial_value.astype(jnp.bfloat16), "tp", scatter_dimension=2, tiled=True
    )
    back = lax.all_to_all(summed, "sp", split_axis=0, concat_axis=0, tiled=True).reshape(
        count * cap, -1
    )
    picked = back[place].reshape(rows, 2, -1).astype(jnp.float32)
    routed = route_weight[:, 0:1] * picked[:, 0] + route_weight[:, 1:2] * picked[:, 1]
    second = depth_scale * settled.astype(jnp.float32) + routed
    sums_two = lax.psum((jnp.sum(second, axis=1), jnp.sum(second * second, axis=1)), "tp")
    return finish_norm(second, sums_two, gain_final, bias_final, columns)


GROUP_COUNT = 4
LANE = 128
BF = jnp.bfloat16
F32 = jnp.float32
LOG2E = 1.4426950408889634


def dot(a, b, dims=((1,), (0,))):
    return lax.dot_general(a, b, (dims, ((), ())), preferred_element_type=F32)


def thirds(v):
    hi = v.astype(BF).astype(F32)
    mid = (v - hi).astype(BF).astype(F32)
    return hi, mid, v - hi - mid


def iota(shape, dim):
    return lax.broadcasted_iota(jnp.int32, shape, dim)


def call(kernel, outs, args, vmem, scratch=(), hidden=0):
    local = pl.BlockSpec(memory_space=pltpu.VMEM)
    spare = pl.BlockSpec(memory_space=pl.ANY)
    return pl.pallas_call(
        kernel,
        out_shape=outs,
        in_specs=[local] * (len(args) - hidden) + [spare] * hidden,
        out_specs=[local] * len(outs),
        scratch_shapes=list(scratch),
        compiler_params=pltpu.CompilerParams(vmem_limit_bytes=vmem << 20),
    )(*args)


def spot():
    sp = lax.axis_index("sp")
    tp = lax.axis_index("tp")
    return sp // 2, sp % 2, tp


def in_hbm(*values):
    return tuple(pltpu.with_memory_space_constraint(v, pltpu.HBM) for v in values)


def shape_of(shape, dtype=BF):
    return jax.ShapeDtypeStruct(shape, dtype)


def route_kernel(cap, ids, weight, *refs):
    m_out, n_out, w_out = refs[-3:]
    z, _, t = spot()
    rows = ids.shape[1]
    first = iota((rows, rows), 0)
    second = iota((rows, rows), 1)

    def column(line):
        return jnp.sum(jnp.where(first == second, line, 0), axis=1, keepdims=True)

    grow = lax.shift_right_logical(ids[0:1, :], 1)
    gcol = column(grow)
    same = gcol == grow
    slot_col = jnp.sum(jnp.where(same & (second < first), 1, 0), axis=1, keepdims=True)
    slot_row = jnp.sum(jnp.where(same & (first < second), 1, 0), axis=0, keepdims=True)
    away = (grow ^ (2 * (z & 1))) ^ t
    block = 2 * (away & 1) + lax.shift_right_logical(away, 1)
    m = jnp.where(iota((4 * cap, rows), 0) == block * cap + slot_row, 1.0, 0.0).astype(BF)
    m_out[...] = m
    place = ((z + 4 - gcol) & 3) * cap + slot_col
    n_out[...] = jnp.where(iota((rows, 4 * cap), 1) == place, 1.0, 0.0).astype(BF)
    even = (ids[0:1, :] & 1) == 0
    w_even = column(jnp.where(even, weight[0:1, :], weight[1:2, :]))
    w_odd = column(jnp.where(even, weight[1:2, :], weight[0:1, :]))
    lane = iota((rows, LANE), 1)
    table = jnp.zeros((rows, LANE), F32)
    for k, part in enumerate(thirds(w_even) + thirds(w_odd)):
        table = jnp.where(lane == k, part, table)
    w_out[...] = dot(m[:cap], table.astype(BF)).astype(BF)


def pack_kernel(qa, ka, qb, kb, offs_a, offs_b, *outs):
    z, x, _ = spot()
    rows = qa.shape[0]
    planes = qa.shape[1] // LANE
    same, cross = outs[:planes], outs[planes:]

    def offset_rows(ref, values):
        parts = []
        for v in values:
            parts += list(thirds(v))
        parts += [jnp.zeros((1, LANE), F32)] * (8 - len(parts))
        block = jnp.concatenate(parts, axis=0).astype(BF)
        for k in range(ref.shape[1] // LANE):
            ref[pl.ds(rows, 8), k * LANE : (k + 1) * LANE] = block

    all_a = ka[...].astype(F32)
    all_b = kb[...].astype(F32)
    for u in range(planes):
        d = (u + planes - z) % planes
        cols = slice(u * LANE, (u + 1) * LANE)
        kv = all_a[:, u, :].astype(BF)
        kv_beta = all_b[:, u, :].astype(BF)
        for k in range(planes):

            @pl.when(d == k)
            def _():
                for flip in range(2):

                    @pl.when(x == flip)
                    def _():
                        alpha, beta = (cross[k], same[k]) if flip else (same[k], cross[k])
                        alpha[0:rows, 0:LANE] = qa[:, cols]
                        alpha[0:rows, LANE : 2 * LANE] = kv
                        offset_rows(alpha, [offs_a[2 * u : 2 * u + 1, :], offs_a[2 * u + 1 : 2 * u + 2, :]])
                        beta[0:rows, 0:LANE] = qb[:, cols]
                        beta[0:rows, LANE : 2 * LANE] = kv_beta[:, 0:LANE]
                        offset_rows(beta, [offs_b[u : u + 1, :]])
                        same[k][0:rows, 2 * LANE :] = kv_beta[:, LANE:]


def relay_kernel(*refs):
    out = refs[-1]
    rows = out.shape[0] // (len(refs) - 1)
    for d, ref in enumerate(refs[:-1]):
        out[d * rows : (d + 1) * rows, :] = ref[0:rows, 2 * LANE :]


def gather_kernel(planes, same, cross, relayed, q_s, k_s, v_s, off_s):
    z, x, _ = spot()
    rows = k_s.shape[0] // (2 * planes)
    half = LANE // 2
    low = iota((rows, LANE), 1) < half
    for d in range(planes):
        for ref, other in ((same[d], x), (cross[d], 1 - x)):
            p = (z + planes - d) % planes
            at = pl.ds(pl.multiple_of((2 * p + other) * rows, rows), rows)
            by_x = pl.ds(pl.multiple_of((planes * other + p) * rows, rows), rows)
            q = ref[0:rows, 0:LANE]
            zero = jnp.zeros_like(q)
            q_s[0, by_x, :] = jnp.where(low | (x != 0), q, zero)
            q_s[1, by_x, :] = jnp.where(low, zero, q)
            kv = ref[0:rows, LANE : 2 * LANE]
            turned = jnp.concatenate([kv[:, half:], kv[:, :half]], axis=1)
            values = relayed[d * rows : (d + 1) * rows, :] if ref is cross[d] else ref[0:rows, 2 * LANE :]
            k_s[at, :] = jnp.where(low | (x != 0), kv, turned)
            v_s[at, :] = jnp.where(x != 0, values, jnp.where(low, turned, kv))
            lines = ref[pl.ds(rows, 8), 0:LANE].astype(F32)
            for h in range(2):
                off_s[h : h + 1, at] = LOG2E * jnp.sum(lines[3 * h : 3 * h + 3], axis=0, keepdims=True)


def attend_half(planes, side, q_s, k_s, v_s, off_s, out, acc_s, rest_s, tri_s):
    z, x, _ = spot()
    rows = k_s.shape[0] // (2 * planes)
    tile = 2 * rows
    low = iota((rows, LANE), 1) < LANE // 2
    ti = iota((tile, tile), 0)
    tj = iota((tile, tile), 1)
    tri_s[...] = jnp.where(ti > tj, 1.0, 0.0).astype(BF)
    valid = (tj < ti + side * rows) | (ti >= rows)
    scale = jnp.where(x == 0, (LANE // 2) ** (-0.5) * LOG2E, LANE ** (-0.5) * LOG2E).astype(F32)
    base = side * (planes * rows)

    def one_head(h, carry):
        for j in range(planes - 1, -1, -1):
            cols = slice(j * tile, (j + 1) * tile)
            first = j * rows
            while first < planes * rows:
                count = min(tile, planes * rows - first)
                at = slice(first, first + count)
                diagonal = first == j * rows
                fresh = rows if diagonal else 0
                q = q_s[h, pl.ds(pl.multiple_of(base + first, rows), count), :]
                s = dot(q, k_s[cols, :], ((1,), (1,))) * scale + off_s[pl.ds(h, 1), cols]
                top = jnp.minimum(s, 64.0)
                take = top - jnp.log2(1.0 + jnp.exp2(top))
                soft = s - take
                if diagonal:
                    soft = jnp.where(valid[:count], soft, 0.0)
                soft = soft.astype(BF)
                after = dot(soft, tri_s[...])
                if fresh:
                    rest_s[first : first + rows, :] = jnp.zeros((rows, 1), F32)
                    acc_s[h, first : first + rows, :] = jnp.zeros((rows, LANE), F32)
                rest = rest_s[at, :]
                w = jnp.exp2(take - (after + rest))
                if diagonal:
                    w = jnp.where(valid[:count], w, 0.0)
                acc_s[h, at, :] = acc_s[h, at, :] + dot(w.astype(BF), v_s[cols, :])
                if j > 0:
                    rest_s[at, :] = rest + after[:, 0:1] + soft[:, 0:1].astype(F32)
                first += count
        return carry

    lax.fori_loop(0, jnp.where(x == 0, 2, 1), one_head, 0)
    for d in range(planes):
        at = pl.ds(pl.multiple_of(((z + d) % planes) * rows, rows), rows)
        value = jnp.where(low | (x != 0), acc_s[0, at, :], acc_s[1, at, :])
        out[d * rows : (d + 1) * rows, :] = value.astype(BF)


def attend_one_kernel(planes, spare, *refs):
    same, cross = refs[:planes], refs[planes : 2 * planes]
    refs = refs[2 * planes :]
    out, *held = refs[1 + spare : 6 + spare]
    gather_kernel(planes, same, cross, refs[0], *held)
    side = 1 - lax.axis_index("sp") % 2
    attend_half(planes, side, *held, out, *refs[6 + spare :])


def attend_two_kernel(planes, *refs):
    attend_half(planes, lax.axis_index("sp") % 2, *refs)


def merge_kernel(own, got, *outs):
    _, x, _ = spot()
    rows = own.shape[0] // len(outs)
    for d, ref in enumerate(outs):
        at = slice(d * rows, (d + 1) * rows)
        ref[:, pl.ds(pl.multiple_of(x * LANE, LANE), LANE)] = own[at]
        ref[:, pl.ds(pl.multiple_of((1 - x) * LANE, LANE), LANE)] = got[at]


def collect_kernel(planes, *refs):
    parts = refs[:planes]
    gains, out, sums = refs[planes:]
    z, _, _ = spot()
    width = planes * LANE
    lane = LANE
    for d in range(planes):
        u = (z + planes - d) % planes
        for k in range(2):
            at = pl.ds(pl.multiple_of(k * width + u * lane, lane), lane)
            out[:, at] = parts[d][:, k * lane : (k + 1) * lane]
    ones = jnp.ones((8, width), F32)
    whole = out[...].astype(F32)
    for k in range(2):
        part = whole[:, k * width : (k + 1) * width]
        line = lax.dot_general(
            ones,
            part * part,
            (((1,), (1,)), ((), ())),
            precision=lax.Precision.HIGHEST,
            preferred_element_type=F32,
        )
        sums[k : k + 1, :] = line[0:1]
    sums[2:8, :] = jnp.zeros((6, sums.shape[1]), F32)
    out[...] = (whole * gains[0:1, :]).astype(BF)


def project_kernel(columns, att, m, resid, s0, s1, s2, s3, pa, pb, keep, send, t_s):
    rows, width = resid.shape
    total = s0[0:2, :] + s1[0:2, :] + s2[0:2, :] + s3[0:2, :]
    factor = lax.rsqrt(total / columns + norm_eps)
    eye = iota((rows, rows), 0) == iota((rows, rows), 1)
    f_a = jnp.sum(jnp.where(eye, factor[0:1], 0.0), axis=1, keepdims=True)
    f_b = jnp.sum(jnp.where(eye, factor[1:2], 0.0), axis=1, keepdims=True)
    for k in range(columns // width):
        at = slice(k * width, (k + 1) * width)
        t_s[:, at] = dot(att[:, :width], pa[:, at]) * f_a + dot(att[:, width:], pb[:, at]) * f_b
    own = pl.ds(pl.multiple_of(lax.axis_index("tp") * width, LANE), width)
    t_s[:, own] = t_s[:, own] + depth_scale * resid[...].astype(F32)
    mid = keep.shape[0]
    for k in range(columns // width):
        at = slice(k * width, (k + 1) * width)
        moved = dot(m[...], t_s[:, at].astype(BF)).astype(BF)
        keep[:, at] = moved[:mid]
        send[:, at] = moved[mid:]


def pair_kernel(keep, got, own, send):
    n = own.shape[0]
    total = keep[...].astype(F32) + got[...].astype(F32)
    own[...] = total[:n]
    send[...] = total[n:].astype(BF)


def settle_kernel(own, got, w, l0, l1, l2, l3, out, lines):
    _, _, t = spot()
    width = l0.shape[1]
    for k, ref in enumerate((l0, l1, l2, l3)):
        lines[:, pl.ds(pl.multiple_of((t ^ k) * width, LANE), width)] = ref[...]
    columns = lines.shape[1]
    first = own[...] + got[...].astype(F32)
    out[:, 0:columns] = row_norm(first, lines[0:1, :], lines[1:2, :])
    out[:, columns : columns + LANE] = w[...]


def row_norm(total, gain, bias):
    columns = total.shape[1]
    mean = jnp.sum(total, axis=1, keepdims=True) / columns
    var = jnp.sum(total * total, axis=1, keepdims=True) / columns - mean * mean
    return ((total - mean) * lax.rsqrt(var + norm_eps) * gain + bias).astype(BF)


def expert_kernel(*refs):
    gate, up, down, near, far, x_s, acc_s, w_s = refs[-8:]
    count = x_s.shape[0] // refs[0].shape[0]
    pieces = refs[:count]
    step = pl.program_id(0)
    n = pieces[0].shape[0]
    columns = x_s.shape[1]

    @pl.when(step == 0)
    def _():
        odd = lax.axis_index("sp") % 2 != 0
        for k in range(count):
            at = slice(k * n, (k + 1) * n)
            x_s[at, :] = pieces[k][:, 0:columns]
            w = pieces[k][:, columns : columns + LANE].astype(F32)
            even_w = w[:, 0:1] + w[:, 1:2] + w[:, 2:3]
            odd_w = w[:, 3:4] + w[:, 4:5] + w[:, 5:6]
            w_s[at, :] = jnp.where(odd, odd_w, even_w)
        acc_s[...] = jnp.zeros_like(acc_s)

    x = x_s[...]
    g = dot(x, gate[0])
    u = dot(x, up[0])
    hidden = (g / (1.0 + jnp.exp(-g)) * u).astype(BF)
    acc_s[...] += dot(hidden, down[0])

    @pl.when(step == pl.num_programs(0) - 1)
    def _():
        mid = count // 2 * n
        width = near.shape[1] // 2
        _, _, t = spot()
        for k in range(2):
            cols = slice(k * width, (k + 1) * width)
            at = pl.ds(pl.multiple_of((t ^ (2 * k)) * width, LANE), width)
            near[:, cols] = (acc_s[:, at] * w_s[...]).astype(BF)
            at = pl.ds(pl.multiple_of((t ^ (2 * k + 1)) * width, LANE), width)
            far[0:mid, cols] = (acc_s[mid:, at] * w_s[mid:, :]).astype(BF)
            far[mid:, cols] = (acc_s[0:mid, at] * w_s[0:mid, :]).astype(BF)


def chip_kernel(spots, targets, near, got, *refs):
    width = near.shape[1] // 2
    count = len(spots)
    n = near.shape[0] // (2 * count)
    for dc in range(2):
        for k, (dx, dy) in enumerate(spots):
            rows = slice((count * dc + k) * n, (count * dc + k + 1) * n)
            for ry in range(2):
                ref = refs[targets.index((dx, ry))]
                cols = slice(ry * width, (ry + 1) * width)
                total = near[rows, cols].astype(F32) + got[rows, cols].astype(F32)
                q = 2 * dc + (dy ^ ry) if ref.shape[0] == 4 * n else dc
                ref[q * n : (q + 1) * n, :] = total.astype(ref.dtype)


def second_kernel(keep, gy, gx0, gx1, gxy0, gxy1, s0, s1, s2, s3, second, sums, routed_s):
    z, _, t = spot()
    n = s0.shape[0]
    width = keep.shape[1]
    at = pl.ds(pl.multiple_of(t * width, LANE), width)
    for q, ref in enumerate((s0, s1, s2, s3)):
        rows = slice(q * n, (q + 1) * n)
        side = slice((q >> 1) * n, ((q >> 1) + 1) * n)
        routed = keep[rows, :] + gy[rows, :].astype(F32)
        for part in (gx1, gxy1) if q & 1 else (gx0, gxy0):
            routed = routed + part[side, :].astype(F32)
        routed_s[rows, :] = routed + depth_scale * ref[:, at].astype(F32)
    for k in range(4):
        dc = (k >> 1) ^ (t & 1)
        dy = ((k & 1) ^ lax.shift_right_logical(z, 1)) ^ lax.shift_right_logical(t, 1)
        start = pl.multiple_of((2 * dc + dy) * n, 16)
        second[k * n : (k + 1) * n, :] = routed_s[pl.ds(start, n), :]
    value = second[...]
    ones = jnp.ones((8, width), F32)
    for k, part in enumerate((value, value * value)):
        line = lax.dot_general(
            ones,
            part,
            (((1,), (1,)), ((), ())),
            precision=lax.Precision.HIGHEST,
            preferred_element_type=F32,
        )
        sums[k : k + 1, 0 : 4 * n] = line[0:1]


def finish_kernel(columns, second, c0, c1, c2, c3, lines, f0, f1, f2, f3, all_s):
    z, _, _ = spot()
    n = f0.shape[0]
    total = c0[0:2, 0 : 4 * n] + c1[0:2, 0 : 4 * n] + c2[0:2, 0 : 4 * n] + c3[0:2, 0 : 4 * n]
    mean = total[0:1] / columns
    scale = lax.rsqrt(total[1:2] / columns - mean * mean + norm_eps)
    eye = iota((4 * n, 4 * n), 0) == iota((4 * n, 4 * n), 1)
    mean = jnp.sum(jnp.where(eye, mean, 0.0), axis=1, keepdims=True)
    scale = jnp.sum(jnp.where(eye, scale, 0.0), axis=1, keepdims=True)
    all_s[...] = ((second[...] - mean) * scale * lines[0:1, :] + lines[1:2, :]).astype(BF)
    for d, ref in enumerate((f0, f1, f2, f3)):
        start = pl.multiple_of(((z + d) & 3) * n, 16)
        ref[...] = all_s[pl.ds(start, n), :]


def load_kernel(*refs):
    count = (len(refs) - 1) // 2
    sems = refs[-1]
    copies = [
        pltpu.make_async_copy(refs[k], refs[count + k], sems.at[k]) for k in range(count)
    ]
    for copy in copies:
        copy.start()
    for copy in copies:
        copy.wait()


def place_kernel(n, f0, f1, f2, f3, out):
    total = dot(n[...], jnp.concatenate([f0[...], f1[...], f2[...], f3[...]], axis=0))
    out[...] = total.astype(BF)


def fast_body(
    chips,
    lanes,
    residual_in,
    query_alpha,
    pairs_alpha,
    offset_alpha,
    gain_alpha,
    query_beta,
    pairs_beta,
    offset_beta,
    gain_beta,
    project_alpha,
    project_beta,
    gain_settle,
    bias_settle,
    expert_ids,
    route_weight,
    expert_gate,
    expert_up,
    expert_down,
    gain_final,
    bias_final,
):
    rows, width = residual_in.shape
    planes = chips // 2
    columns = width * lanes
    cap = 3 * rows // chips

    def move(v, dest):
        perm = []
        for a in range(chips * lanes):
            s, t = divmod(a, lanes)
            to = dest(s // 2, s % 2, t)
            if to is not None:
                perm.append((a, (to[0] * 2 + to[1]) * lanes + to[2]))
        return lax.ppermute(v, ("sp", "tp"), perm)

    def shift(v, d, flip):
        return move(v, lambda z, x, t: ((z + d) % planes, x ^ flip, t))

    def swap_tp(v, k):
        return move(v, lambda z, x, t: (z, x, t ^ k))

    def across_tp(v):
        other_y = swap_tp(v, 2)
        return v, swap_tp(v, 1), other_y, swap_tp(other_y, 1)

    def swap_plane(v, dx, k):
        return move(v, lambda z, x, t: (z, x ^ dx, t ^ k))

    packed = call(
        pack_kernel,
        [shape_of((rows + 8, 3 * LANE))] * planes + [shape_of((rows + 8, 2 * LANE))] * planes,
        in_hbm(
            query_alpha,
            pairs_alpha,
            query_beta,
            pairs_beta,
            jnp.transpose(offset_alpha),
            jnp.transpose(offset_beta),
        ),
        12,
    )
    same, cross = packed[:planes], packed[planes:]
    got_same, got_cross = [same[0]] + [None] * (planes - 1), [None] * planes
    for d in (2, 1, 3):
        got_same[d] = shift(same[d], d, 0)
    for d in (2, 1, 3, 0):
        got_cross[d] = shift(cross[d], d, 1)
    (values,) = call(relay_kernel, [shape_of((planes * rows, LANE))], got_same, 4)
    relayed = swap_plane(values, 1, 0)

    m, n, w = call(
        lambda *refs: route_kernel(cap, *refs),
        [shape_of((4 * cap, rows)), shape_of((rows, 4 * cap)), shape_of((cap, LANE))],
        (*in_hbm(jnp.transpose(expert_ids), jnp.transpose(route_weight)), got_same[2]),
        8,
        hidden=1,
    )
    own_lines = jnp.stack([gain_settle, bias_settle])
    lines = [own_lines] + [swap_tp(own_lines, k) for k in range(1, 4)]

    def load(weights, after):
        count = len(weights)
        anywhere = pl.BlockSpec(memory_space=pl.ANY)
        return pl.pallas_call(
            lambda *refs: load_kernel(*refs[:count], *refs[count + 1 :]),
            out_shape=[shape_of(v.shape) for v in weights],
            in_specs=[anywhere] * (count + 1),
            out_specs=[pl.BlockSpec(memory_space=pltpu.VMEM)] * count,
            scratch_shapes=[pltpu.SemaphoreType.DMA((count,))],
            compiler_params=pltpu.CompilerParams(vmem_limit_bytes=16 << 20),
        )(*in_hbm(*weights), after)

    p_alpha, p_beta = load((project_alpha, project_beta), got_same[2])

    total = chips * rows
    spare = (m, n, w, *lines[1:], p_alpha)
    work = [
        pltpu.VMEM((2, planes * rows, LANE), F32),
        pltpu.VMEM((planes * rows, 1), F32),
        pltpu.VMEM((2 * rows, 2 * rows), BF),
    ]
    half = shape_of((planes * rows, LANE))
    other_x, *held = call(
        lambda *refs: attend_one_kernel(planes, len(spare), *refs),
        [half, shape_of((2, total, LANE)), shape_of((total, LANE)), shape_of((total, LANE)), shape_of((8, total), F32)],
        (*got_same, *got_cross, relayed, *spare),
        12,
        hidden=len(spare),
        scratch=work,
    )
    got_x = swap_plane(other_x, 1, 0)
    (own_x,) = call(
        lambda *refs: attend_two_kernel(planes, *refs), [half], tuple(held), 12, scratch=work
    )
    merged = call(merge_kernel, [shape_of((rows, 2 * LANE))] * planes, (own_x, got_x), 4)
    back = [merged[0]] + [shift(merged[d], d, 0) for d in range(1, planes)]
    gains = jnp.concatenate([gain_alpha, gain_beta])[None, :]
    att, sums = call(
        lambda *refs: collect_kernel(planes, *refs),
        [shape_of((rows, 2 * width)), shape_of((8, rows), F32)],
        (*back, gains),
        8,
    )
    all_sums = across_tp(sums)

    keep, send = call(
        lambda *refs: project_kernel(columns, *refs),
        [shape_of((2 * cap, columns))] * 2,
        (att, m, *in_hbm(residual_in), *all_sums, p_alpha, p_beta),
        12,
        scratch=[pltpu.VMEM((rows, columns), F32)],
    )
    own, send = call(
        pair_kernel,
        [shape_of((cap, columns), F32), shape_of((cap, columns))],
        (keep, swap_tp(send, 1)),
        8,
    )
    got = swap_tp(send, 2)
    e_gate, e_up, e_down = load((expert_gate, expert_up, expert_down), keep)
    settled, _ = call(
        settle_kernel,
        [shape_of((cap, columns + LANE)), shape_of((2, columns), F32)],
        (own, got, w, *lines),
        8,
    )

    def to_plane(z, x, t):
        g = t ^ (2 * (z & 1))
        return g, x, 2 * (t >> 1) + (z >> 1)

    mine = move(settled, to_plane)
    from_x, from_y, from_xy = (
        swap_plane(mine, 1, 0),
        swap_plane(mine, 0, 2),
        swap_plane(mine, 1, 2),
    )
    near = [mine, from_x, from_y]
    far = [swap_plane(mine, 0, 1)] + [swap_plane(v, 0, 1) for v in near[1:]]
    hidden = expert_gate.shape[2]
    chunk = hidden // 2

    def experts(pieces):
        n = len(pieces) * cap
        out = pl.BlockSpec((n, 2 * width), lambda j: (0, 0))
        return pl.pallas_call(
            expert_kernel,
            grid=(hidden // chunk,),
            out_shape=[shape_of((n, 2 * width))] * 2,
            in_specs=[pl.BlockSpec((cap, columns + LANE), lambda j: (0, 0))] * len(pieces)
            + [
                pl.BlockSpec((1, columns, chunk), lambda j: (0, 0, j)),
                pl.BlockSpec((1, columns, chunk), lambda j: (0, 0, j)),
                pl.BlockSpec((1, chunk, columns), lambda j: (0, j, 0)),
            ],
            out_specs=[out] * 2,
            scratch_shapes=[
                pltpu.VMEM((n, columns), BF),
                pltpu.VMEM((n, columns), F32),
                pltpu.VMEM((n, 1), F32),
            ],
            compiler_params=pltpu.CompilerParams(vmem_limit_bytes=24 << 20),
        )(*pieces, e_gate, e_up, e_down)

    def chip(spots, targets, outs, own, got):
        kernel = lambda *refs: chip_kernel(spots, targets, *refs)
        return call(kernel, outs, (own, got), 8)

    whole, side = shape_of((4 * cap, width)), shape_of((2 * cap, width))
    near_one, far_one = experts(near + far)
    keep, to_y, to_x0, to_xy0 = chip(
        ((0, 0), (1, 0), (0, 1)),
        ((0, 0), (0, 1), (1, 0), (1, 1)),
        [shape_of(whole.shape, F32), whole, side, side],
        near_one,
        swap_plane(far_one, 0, 1),
    )
    last, _ = lax.optimization_barrier((from_xy, far_one))
    near_two, far_two = experts([last, swap_plane(last, 0, 1)])
    to_x1, to_xy1 = chip(
        ((1, 1),), ((1, 0), (1, 1)), [side, side], near_two, swap_plane(far_two, 0, 1)
    )
    got_y = swap_plane(to_y, 0, 2)
    got_x0, got_x1 = swap_plane(to_x0, 1, 0), swap_plane(to_x1, 1, 0)
    got_xy1, got_xy0 = swap_plane(to_xy0, 1, 2), swap_plane(to_xy1, 1, 2)
    second, sums = call(
        second_kernel,
        [shape_of((4 * cap, width), F32), shape_of((8, 2 * LANE), F32)],
        (keep, got_y, got_x0, got_x1, got_xy0, got_xy1, near[0], near[2], far[0], far[2]),
        8,
        scratch=[pltpu.VMEM((4 * cap, width), F32)],
    )
    all_sums = across_tp(sums)
    ends = call(
        lambda *refs: finish_kernel(columns, *refs),
        [shape_of((cap, width))] * planes,
        (second, *all_sums, jnp.stack([gain_final, bias_final])),
        8,
        scratch=[pltpu.VMEM((4 * cap, width), BF)],
    )
    home = [ends[0]] + [shift(ends[d], d, 0) for d in range(1, planes)]
    (out,) = call(place_kernel, [shape_of((rows, width))], (n, *home), 4)
    return out


def solution(mesh):
    chips, lanes = mesh.shape["sp"], mesh.shape["tp"]

    def body(*args):
        residual_in, pairs_alpha, pairs_beta = args[0], args[2], args[6]
        planes = chips // 2
        fast = (
            chips // GROUP_COUNT == 2
            and lanes == planes
            and lanes == 4
            and pairs_alpha.shape[1] == planes
            and pairs_beta.shape[1] == planes
            and pairs_alpha.shape[2] == LANE
            and pairs_beta.shape[2] == 2 * LANE
            and residual_in.shape[0] == LANE
            and args[1].shape[1] == planes * LANE
            and args[5].shape[1] == planes * LANE
        )
        if not fast:
            return general_body(*args)
        return fast_body(chips, lanes, *args)

    in_specs = (
        P("sp", "tp"),
        P("sp", "tp"),
        P("sp", "tp", None),
        P("sp", "tp"),
        P("tp"),
        P("sp", "tp"),
        P("sp", "tp", None),
        P("sp", "tp"),
        P("tp"),
        P("tp", None),
        P("tp", None),
        P("tp"),
        P("tp"),
        P("sp", None),
        P("sp", None),
        P("sp", None, "tp"),
        P("sp", None, "tp"),
        P("sp", "tp", None),
        P("tp"),
        P("tp"),
    )
    out_specs = P("sp", "tp")
    return jax.shard_map(body, mesh=mesh, in_specs=in_specs, out_specs=out_specs, check_vma=False)
```

profile of v0, /device:TPU:0, one launch (start us, length us, event | category | flops | bytes accessed | tf_op | source)
XLA Modules:
  0.0 133.9 jit_solution(8891059387935689135)
XLA Ops:
  0.0 2.3 %shard_map.190 = (bf16[136,384]{1,0:T(8,128)(2,1)S(1)}, bf16[136,384]{1,0:T(8,128)(2,1)S(1)}, bf16[136,384]{1,0:T(8,128)(2,1)S(1)}, bf16[136,384]{1,0:T(8,128)(2...) custom-call(bf16[128,512]{1,0:T(8,128)(2,1)} %qa.1, ...), custom_call_target="tpu_custom_call" | custom-call | tf_op jit(solution)/shard_map/pallas_call | solution.py:203
  2.3 4.1 %collective-permute-start = (bf16[136,384]{1,0:T(8,128)(2,1)S(1)}, bf16[136,384]{1,0:T(8,128)(2,1)S(1)}, u32[]{:S(2)}, u32[]{:S(2)}) collective-permute-start(bf16[136,384]{1,0:T(8,128)(2,1)S(1)} %get-tuple-element.54), channel_id=1, source_target_pairs={{0,16},{1,17},{2,18},{3,19},{4,20},{5,21},{6,22},{7,23},{8,24},{9,... | collective-permute-start | bytes 313352 | tf_op jit(solution)/shard_map/ppermute | solution.py:626
  8.1 2.2 %collective-permute-start.2 = (bf16[136,384]{1,0:T(8,128)(2,1)S(1)}, bf16[136,384]{1,0:T(8,128)(2,1)S(1)}, u32[]{:S(2)}, u32[]{:S(2)}) collective-permute-start(bf16[136,384]{1,0:T(8,128)(2,1)S(1)} %get-tuple-element.58), channel_id=1, source_target_pairs={{0,24},{1,25},{2,26},{3,27},{4,28},{5,29},{6,30},{7,31},{8,0},{9,1... | collective-permute-start | bytes 313352 | tf_op jit(solution)/shard_map/ppermute | solution.py:626
  10.3 4.5 %collective-permute-done.refs_2_ = bf16[136,384]{1,0:T(8,128)(2,1)S(1)} collective-permute-done((bf16[136,384]{1,0:T(8,128)(2,1)S(1)}, bf16[136,384]{1,0:T(8,128)(2,1)S(1)}, u32[]{:S(2)}, u32[]{:S(2)}) %collective-permute-start) | collective-permute-done | bytes 104480 | tf_op jit(solution)/shard_map/ppermute | solution.py:626
  15.5 1.6 %collective-permute-start.7 = (bf16[512,128]{1,0:T(8,128)(2,1)S(1)}, bf16[512,128]{1,0:T(8,128)(2,1)S(1)}, u32[]{:S(2)}, u32[]{:S(2)}) collective-permute-start(bf16[512,128]{1,0:T(8,128)(2,1)S(1)} %shard_map.192), channel_id=1, source_target_pairs={{0,4},{1,5},{2,6},{3,7},{4,0},{5,1},{6,2},{7,3},{8,12},{9,13},{10,... | collective-permute-start | bytes 393224 | tf_op jit(solution)/shard_map/ppermute | solution.py:626
  17.9 1.6 %collective-permute-start.8 = (f32[2,512]{1,0:T(2,128)S(1)}, f32[2,512]{1,0:T(2,128)S(1)}, u32[]{:S(2)}, u32[]{:S(2)}) collective-permute-start(f32[2,512]{1,0:T(2,128)S(1)} %pad_maximum_fusion.l0), channel_id=1, source_target_pairs={{0,1},{1,0},{2,3},{3,2},{4,5},{5,4},{6,7},{7,6},{8,9},{9,8},{10,11... | collective-permute-start | bytes 12296 | tf_op jit(solution)/shard_map/ppermute | solution.py:626
  20.9 1.9 %collective-permute-start.4 = (bf16[136,256]{1,0:T(8,128)(2,1)S(1)}, bf16[136,256]{1,0:T(8,128)(2,1)S(1)}, u32[]{:S(2)}, u32[]{:S(2)}) collective-permute-start(bf16[136,256]{1,0:T(8,128)(2,1)S(1)} %get-tuple-element.60), channel_id=1, source_target_pairs={{0,12},{1,13},{2,14},{3,15},{4,8},{5,9},{6,10},{7,11},{8,20},{9,21... | collective-permute-start | bytes 208904 | tf_op jit(solution)/shard_map/ppermute | solution.py:626
  22.8 2.0 %collective-permute-start.5 = (bf16[136,256]{1,0:T(8,128)(2,1)S(1)}, bf16[136,256]{1,0:T(8,128)(2,1)S(1)}, u32[]{:S(2)}, u32[]{:S(2)}) collective-permute-start(bf16[136,256]{1,0:T(8,128)(2,1)S(1)} %get-tuple-element.61), channel_id=1, source_target_pairs={{0,20},{1,21},{2,22},{3,23},{4,16},{5,17},{6,18},{7,19},{8,28},{9,... | collective-permute-start | bytes 208904 | tf_op jit(solution)/shard_map/ppermute | solution.py:626
  24.8 3.8 %collective-permute-start.6 = (bf16[136,256]{1,0:T(8,128)(2,1)S(1)}, bf16[136,256]{1,0:T(8,128)(2,1)S(1)}, u32[]{:S(2)}, u32[]{:S(2)}) collective-permute-start(bf16[136,256]{1,0:T(8,128)(2,1)S(1)} %get-tuple-element.62), channel_id=1, source_target_pairs={{0,28},{1,29},{2,30},{3,31},{4,24},{5,25},{6,26},{7,27},{8,4},{9,5... | collective-permute-start | bytes 208904 | tf_op jit(solution)/shard_map/ppermute | solution.py:626
  29.5 2.3 %shard_map.193 = (bf16[512,2048]{1,0:T(8,128)(2,1)S(1)}, bf16[512,2048]{1,0:T(8,128)(2,1)S(1)}) custom-call(bf16[512,2048]{1,0:T(8,128)(2,1)} %refs_0_.2, bf16[512,2048]{1,0:T(8,128)(2,1)} %refs_1_.2, bf16[136,384]{1,0:T(8,128)(2,1)S(1)} %collective-permute-done.refs_2_), custom_call_target="tpu_custom_call" | custom-call | tf_op jit(solution)/shard_map/pallas_call | solution.py:676
  31.9 3.5 %shard_map.194 = (bf16[512,128]{1,0:T(8,128)(2,1)S(1)}, bf16[2,1024,128]{2,1,0:T(8,128)(2,1)S(1)}, bf16[1024,128]{1,0:T(8,128)(2,1)S(1)}, bf16[1024,128]{1,0:T(8,128)(2,1)S(1)}, f32[8,1024]{1,0:T(8,128)S(1)}) custom-call(bf16[136,384]{1,0:T(8,128)(2,1)S(1)} %get-tuple-element.56.refs_0_, bf16[136,384]{1,0:T(8,128)(2,1)S(1)} %collective-permute-done.1.refs_1_, ...), custom_call_target="tpu_custom_call" | custom-call | tf_op jit(solution)/shard_map/pallas_call | solution.py:203
  35.5 3.2 %shard_map.195.own = bf16[512,128]{1,0:T(8,128)(2,1)S(1)} custom-call(bf16[2,1024,128]{2,1,0:T(8,128)(2,1)S(1)} %get-tuple-element.66.refs_0_, bf16[1024,128]{1,0:T(8,128)(2,1)S(1)} %get-tuple-element.67.refs_1_, bf16[1024,128]{1,0:T(8,128)(2,1)S(1)} %get-tuple-element.68.refs_2_, f32[8,1024]{1,0:T(8,128)S(1)} %get-tuple-element.69.refs_3_), custom_call_target="tpu_custom_call" | custom-call | tf_op jit(solution)/shard_map/pallas_call | solution.py:203
  38.7 1.7 %collective-permute-done.11.got = bf16[512,128]{1,0:T(8,128)(2,1)S(1)} collective-permute-done((bf16[512,128]{1,0:T(8,128)(2,1)S(1)}, bf16[512,128]{1,0:T(8,128)(2,1)S(1)}, u32[]{:S(2)}, u32[]{:S(2)}) %collective-permute-start.11) | collective-permute-done | bytes 131104 | tf_op jit(solution)/shard_map/ppermute | solution.py:626
  41.7 2.5 %collective-permute-start.13 = (bf16[128,256]{1,0:T(8,128)(2,1)S(1)}, bf16[128,256]{1,0:T(8,128)(2,1)S(1)}, u32[]{:S(2)}, u32[]{:S(2)}) collective-permute-start(bf16[128,256]{1,0:T(8,128)(2,1)S(1)} %get-tuple-element.73), channel_id=1, source_target_pairs={{0,16},{1,17},{2,18},{3,19},{4,20},{5,21},{6,22},{7,23},{8,24},{9,... | collective-permute-start | bytes 196616 | tf_op jit(solution)/shard_map/ppermute | solution.py:626
  44.4 2.3 %collective-permute-done.12.refs_1_ = bf16[128,256]{1,0:T(8,128)(2,1)S(1)} collective-permute-done((bf16[128,256]{1,0:T(8,128)(2,1)S(1)}, bf16[128,256]{1,0:T(8,128)(2,1)S(1)}, u32[]{:S(2)}, u32[]{:S(2)}) %collective-permute-start.12) | collective-permute-done | bytes 65568 | tf_op jit(solution)/shard_map/ppermute | solution.py:626
  50.7 2.2 %collective-permute-done.16.refs_5_ = f32[8,128]{1,0:T(8,128)S(1)} collective-permute-done((f32[8,128]{1,0:T(8,128)S(1)}, f32[8,128]{1,0:T(8,128)S(1)}, u32[]{:S(2)}, u32[]{:S(2)}) %collective-permute-start.16) | collective-permute-done | bytes 4128 | tf_op jit(solution)/shard_map/ppermute | solution.py:626
  54.1 2.1 %shard_map.198 = (bf16[96,2048]{1,0:T(8,128)(2,1)S(1)}, bf16[96,2048]{1,0:T(8,128)(2,1)S(1)}) custom-call(bf16[128,1024]{1,0:T(8,128)(2,1)S(1)} %get-tuple-element.75.refs_0_, bf16[192,128]{1,0:T(8,128)(2,1)S(1)} %get-tuple-element.63.refs_9_.refs_1_, bf16[128,512]{1,0:T(8,128)(2,1)} %refs_2_.2, f32[8,128]{1,0:T(8,128)S(1)} %get-tuple-element.76.refs_3_, ...), custom_call_target="tpu_custom_call" | custom-call | tf_op jit(solution)/shard_map/pallas_call | solution.py:203
  59.5 5.6 %collective-permute-done.19.got = bf16[48,2048]{1,0:T(8,128)(2,1)S(1)} collective-permute-done((bf16[48,2048]{1,0:T(8,128)(2,1)S(1)}, bf16[48,2048]{1,0:T(8,128)(2,1)S(1)}, u32[]{:S(2)}, u32[]{:S(2)}) %collective-permute-start.19) | collective-permute-done | bytes 196640 | tf_op jit(solution)/shard_map/ppermute | solution.py:626
  66.9 10.2 %collective-permute-start.22 = (bf16[48,2176]{1,0:T(8,128)(2,1)S(1)}, bf16[48,2176]{1,0:T(8,128)(2,1)S(1)}, u32[]{:S(2)}, u32[]{:S(2)}) collective-permute-start(bf16[48,2176]{1,0:T(8,128)(2,1)S(1)} %collective-permute-done.20.refs_0_.s0), channel_id=1, source_target_pairs={{0,2},{1,3},{2,0},{3,1},{4,6},{5,7},{6,4},{7,5},{8,10},{9,11},{10,... | collective-permute-start | bytes 626696 | tf_op jit(solution)/shard_map/ppermute | solution.py:626
  77.1 1.7 %collective-permute-start.24 = (bf16[48,2176]{1,0:T(8,128)(2,1)S(1)}, bf16[48,2176]{1,0:T(8,128)(2,1)S(1)}, u32[]{:S(2)}, u32[]{:S(2)}) collective-permute-start(bf16[48,2176]{1,0:T(8,128)(2,1)S(1)} %collective-permute-done.21.refs_1_), channel_id=1, source_target_pairs={{0,1},{1,0},{2,3},{3,2},{4,5},{5,4},{6,7},{7,6},{8,9},{9,8},{10,11... | collective-permute-start | bytes 626696 | tf_op jit(solution)/shard_map/ppermute | solution.py:626
  78.8 2.8 %collective-permute-done.22.refs_2_.s1 = bf16[48,2176]{1,0:T(8,128)(2,1)S(1)} collective-permute-done((bf16[48,2176]{1,0:T(8,128)(2,1)S(1)}, bf16[48,2176]{1,0:T(8,128)(2,1)S(1)}, u32[]{:S(2)}, u32[]{:S(2)}) %collective-permute-start.22) | collective-permute-done | bytes 208928 | tf_op jit(solution)/shard_map/ppermute | solution.py:626
  81.6 4.7 %shard_map.201 = (bf16[1,2048,1024]{2,1,0:T(8,128)(2,1)S(1)}, bf16[1,2048,1024]{2,1,0:T(8,128)(2,1)S(1)}, bf16[1,1024,2048]{2,1,0:T(8,128)(2,1)S(1)}) custom-call(bf16[1,2048,1024]{2,1,0:T(8,128)(2,1)} %refs_0_.3, bf16[1,2048,1024]{2,1,0:T(8,128)(2,1)} %refs_1_.3, bf16[1,1024,2048]{2,1,0:T(8,128)(2,1)} %refs_2_.3, ...), custom_call_target="tpu_custom_call" | custom-call | tf_op jit(solution)/shard_map/pallas_call | solution.py:676
  86.3 5.3 %shard_map.202 = (bf16[288,1024]{1,0:T(8,128)(2,1)S(1)}, bf16[288,1024]{1,0:T(8,128)(2,1)S(1)}) custom-call(bf16[48,2176]{1,0:T(8,128)(2,1)S(1)} %collective-permute-done.20.refs_0_.s0, bf16[48,2176]{1,0:T(8,128)(2,1)S(1)} %collective-permute-done.21.refs_1_, bf16[48,2176]{1,0:T(8,128)(2,1)S(1)} %collective-permute-done.22.refs_2_.s1, ...), custom_call_target="tpu_custom_call" | custom-call | tf_op jit(solution)/shard_map/pallas_call | solution.py:758
  92.2 2.9 %collective-permute-start.29 = (bf16[48,2176]{1,0:T(8,128)(2,1)S(1)}, bf16[48,2176]{1,0:T(8,128)(2,1)S(1)}, u32[]{:S(2)}, u32[]{:S(2)}) collective-permute-start(bf16[48,2176]{1,0:T(8,128)(2,1)S(1)} %collective-permute-done.20.refs_0_.s0), channel_id=1, source_target_pairs={{0,6},{1,7},{2,4},{3,5},{4,2},{5,3},{6,0},{7,1},{8,14},{9,15},{10,... | collective-permute-start | bytes 626696 | tf_op jit(solution)/shard_map/ppermute | solution.py:626
  95.2 5.4 %collective-permute-done.29.refs_0_ = bf16[48,2176]{1,0:T(8,128)(2,1)S(1)} collective-permute-done((bf16[48,2176]{1,0:T(8,128)(2,1)S(1)}, bf16[48,2176]{1,0:T(8,128)(2,1)S(1)}, u32[]{:S(2)}, u32[]{:S(2)}) %collective-permute-start.29) | collective-permute-done | bytes 208928 | tf_op jit(solution)/shard_map/ppermute | solution.py:626
  102.0 3.4 %shard_map.204 = (bf16[96,1024]{1,0:T(8,128)(2,1)S(1)}, bf16[96,1024]{1,0:T(8,128)(2,1)S(1)}) custom-call(bf16[48,2176]{1,0:T(8,128)(2,1)S(1)} %collective-permute-done.29.refs_0_, bf16[48,2176]{1,0:T(8,128)(2,1)S(1)} %collective-permute-done.30.refs_1_, bf16[1,2048,1024]{2,1,0:T(8,128)(2,1)S(1)} %get-tuple-element.83.refs_6_.refs_2_, ...), custom_call_target="tpu_custom_call" | custom-call | tf_op jit(solution)/shard_map/pallas_call | solution.py:758
  105.8 1.9 %collective-permute-start.27 = (bf16[192,512]{1,0:T(8,128)(2,1)S(1)}, bf16[192,512]{1,0:T(8,128)(2,1)S(1)}, u32[]{:S(2)}, u32[]{:S(2)}) collective-permute-start(bf16[192,512]{1,0:T(8,128)(2,1)S(1)} %get-tuple-element.89), channel_id=1, source_target_pairs={{0,2},{1,3},{2,0},{3,1},{4,6},{5,7},{6,4},{7,5},{8,10},{9,11},{10,... | collective-permute-start | bytes 589832 | tf_op jit(solution)/shard_map/ppermute | solution.py:626
  113.1 3.0 %collective-permute-done.33.gxy0 = bf16[96,512]{1,0:T(8,128)(2,1)S(1)} collective-permute-done((bf16[96,512]{1,0:T(8,128)(2,1)S(1)}, bf16[96,512]{1,0:T(8,128)(2,1)S(1)}, u32[]{:S(2)}, u32[]{:S(2)}) %collective-permute-start.33) | collective-permute-done | bytes 98336 | tf_op jit(solution)/shard_map/ppermute | solution.py:626
  117.5 2.0 %collective-permute-done.34.gxy1 = bf16[96,512]{1,0:T(8,128)(2,1)S(1)} collective-permute-done((bf16[96,512]{1,0:T(8,128)(2,1)S(1)}, bf16[96,512]{1,0:T(8,128)(2,1)S(1)}, u32[]{:S(2)}, u32[]{:S(2)}) %collective-permute-start.34) | collective-permute-done | bytes 98336 | tf_op jit(solution)/shard_map/ppermute | solution.py:626
  121.3 2.7 %collective-permute-done.36.refs_3_ = f32[8,256]{1,0:T(8,128)S(1)} collective-permute-done((f32[8,256]{1,0:T(8,128)S(1)}, f32[8,256]{1,0:T(8,128)S(1)}, u32[]{:S(2)}, u32[]{:S(2)}) %collective-permute-start.36) | collective-permute-done | bytes 8224 | tf_op jit(solution)/shard_map/ppermute | solution.py:626
  125.5 2.7 %collective-permute-start.39 = (bf16[48,512]{1,0:T(8,128)(2,1)S(1)}, bf16[48,512]{1,0:T(8,128)(2,1)S(1)}, u32[]{:S(2)}, u32[]{:S(2)}) collective-permute-start(bf16[48,512]{1,0:T(8,128)(2,1)S(1)} %get-tuple-element.101), channel_id=1, source_target_pairs={{0,16},{1,17},{2,18},{3,19},{4,20},{5,21},{6,22},{7,23},{8,24},{9,... | collective-permute-start | bytes 147464 | tf_op jit(solution)/shard_map/ppermute | solution.py:626
  129.3 2.6 %collective-permute-done.38.f1 = bf16[48,512]{1,0:T(8,128)(2,1)S(1)} collective-permute-done((bf16[48,512]{1,0:T(8,128)(2,1)S(1)}, bf16[48,512]{1,0:T(8,128)(2,1)S(1)}, u32[]{:S(2)}, u32[]{:S(2)}) %collective-permute-start.38) | collective-permute-done | bytes 49184 | tf_op jit(solution)/shard_map/ppermute | solution.py:626
  (80 shorter events, 32.8 us)
Async XLA Ops:
  2.3 12.4 %collective-permute-start = (bf16[136,384]{1,0:T(8,128)(2,1)S(1)}, bf16[136,384]{1,0:T(8,128)(2,1)S(1)}, u32[]{:S(2)}, u32[]{:S(2)}) collective-permute-start(bf16[136,384]{1,0:T(8,128)(2,1)S(1)} %get-tuple-element.54), channel_id=1, source_target_pairs={{0,16},{1,17},{2,18},{3,19},{4,20},{5,21},{6,22},{7,23},{8,24},{9,... | collective-permute-start | bytes 313352 | tf_op jit(solution)/shard_map/ppermute | solution.py:626
  6.5 8.3 %collective-permute-start.1 = (bf16[136,384]{1,0:T(8,128)(2,1)S(1)}, bf16[136,384]{1,0:T(8,128)(2,1)S(1)}, u32[]{:S(2)}, u32[]{:S(2)}) collective-permute-start(bf16[136,384]{1,0:T(8,128)(2,1)S(1)} %get-tuple-element.57), channel_id=1, source_target_pairs={{0,8},{1,9},{2,10},{3,11},{4,12},{5,13},{6,14},{7,15},{8,16},{9,17... | collective-permute-start | bytes 313352 | tf_op jit(solution)/shard_map/ppermute | solution.py:626
  8.1 7.4 %collective-permute-start.2 = (bf16[136,384]{1,0:T(8,128)(2,1)S(1)}, bf16[136,384]{1,0:T(8,128)(2,1)S(1)}, u32[]{:S(2)}, u32[]{:S(2)}) collective-permute-start(bf16[136,384]{1,0:T(8,128)(2,1)S(1)} %get-tuple-element.58), channel_id=1, source_target_pairs={{0,24},{1,25},{2,26},{3,27},{4,28},{5,29},{6,30},{7,31},{8,0},{9,1... | collective-permute-start | bytes 313352 | tf_op jit(solution)/shard_map/ppermute | solution.py:626
  15.5 16.3 %collective-permute-start.7 = (bf16[512,128]{1,0:T(8,128)(2,1)S(1)}, bf16[512,128]{1,0:T(8,128)(2,1)S(1)}, u32[]{:S(2)}, u32[]{:S(2)}) collective-permute-start(bf16[512,128]{1,0:T(8,128)(2,1)S(1)} %shard_map.192), channel_id=1, source_target_pairs={{0,4},{1,5},{2,6},{3,7},{4,0},{5,1},{6,2},{7,3},{8,12},{9,13},{10,... | collective-permute-start | bytes 393224 | tf_op jit(solution)/shard_map/ppermute | solution.py:626
  17.9 4.9 %collective-permute-start.8 = (f32[2,512]{1,0:T(2,128)S(1)}, f32[2,512]{1,0:T(2,128)S(1)}, u32[]{:S(2)}, u32[]{:S(2)}) collective-permute-start(f32[2,512]{1,0:T(2,128)S(1)} %pad_maximum_fusion.l0), channel_id=1, source_target_pairs={{0,1},{1,0},{2,3},{3,2},{4,5},{5,4},{6,7},{7,6},{8,9},{9,8},{10,11... | collective-permute-start | bytes 12296 | tf_op jit(solution)/shard_map/ppermute | solution.py:626
  19.5 5.3 %collective-permute-start.9 = (f32[2,512]{1,0:T(2,128)S(1)}, f32[2,512]{1,0:T(2,128)S(1)}, u32[]{:S(2)}, u32[]{:S(2)}) collective-permute-start(f32[2,512]{1,0:T(2,128)S(1)} %pad_maximum_fusion.l0), channel_id=1, source_target_pairs={{0,2},{1,3},{2,0},{3,1},{4,6},{5,7},{6,4},{7,5},{8,10},{9,11},{10,... | collective-permute-start | bytes 12296 | tf_op jit(solution)/shard_map/ppermute | solution.py:626
  20.0 11.8 %collective-permute-start.3 = (bf16[136,256]{1,0:T(8,128)(2,1)S(1)}, bf16[136,256]{1,0:T(8,128)(2,1)S(1)}, u32[]{:S(2)}, u32[]{:S(2)}) collective-permute-start(bf16[136,256]{1,0:T(8,128)(2,1)S(1)} %get-tuple-element.59), channel_id=1, source_target_pairs={{0,4},{1,5},{2,6},{3,7},{4,0},{5,1},{6,2},{7,3},{8,12},{9,13},{10,... | collective-permute-start | bytes 208904 | tf_op jit(solution)/shard_map/ppermute | solution.py:626
  20.9 10.9 %collective-permute-start.4 = (bf16[136,256]{1,0:T(8,128)(2,1)S(1)}, bf16[136,256]{1,0:T(8,128)(2,1)S(1)}, u32[]{:S(2)}, u32[]{:S(2)}) collective-permute-start(bf16[136,256]{1,0:T(8,128)(2,1)S(1)} %get-tuple-element.60), channel_id=1, source_target_pairs={{0,12},{1,13},{2,14},{3,15},{4,8},{5,9},{6,10},{7,11},{8,20},{9,21... | collective-permute-start | bytes 208904 | tf_op jit(solution)/shard_map/ppermute | solution.py:626
  22.8 9.0 %collective-permute-start.5 = (bf16[136,256]{1,0:T(8,128)(2,1)S(1)}, bf16[136,256]{1,0:T(8,128)(2,1)S(1)}, u32[]{:S(2)}, u32[]{:S(2)}) collective-permute-start(bf16[136,256]{1,0:T(8,128)(2,1)S(1)} %get-tuple-element.61), channel_id=1, source_target_pairs={{0,20},{1,21},{2,22},{3,23},{4,16},{5,17},{6,18},{7,19},{8,28},{9,... | collective-permute-start | bytes 208904 | tf_op jit(solution)/shard_map/ppermute | solution.py:626
  24.8 7.0 %collective-permute-start.6 = (bf16[136,256]{1,0:T(8,128)(2,1)S(1)}, bf16[136,256]{1,0:T(8,128)(2,1)S(1)}, u32[]{:S(2)}, u32[]{:S(2)}) collective-permute-start(bf16[136,256]{1,0:T(8,128)(2,1)S(1)} %get-tuple-element.62), channel_id=1, source_target_pairs={{0,28},{1,29},{2,30},{3,31},{4,24},{5,25},{6,26},{7,27},{8,4},{9,5... | collective-permute-start | bytes 208904 | tf_op jit(solution)/shard_map/ppermute | solution.py:626
  35.4 5.0 %collective-permute-start.11 = (bf16[512,128]{1,0:T(8,128)(2,1)S(1)}, bf16[512,128]{1,0:T(8,128)(2,1)S(1)}, u32[]{:S(2)}, u32[]{:S(2)}) collective-permute-start(bf16[512,128]{1,0:T(8,128)(2,1)S(1)} %get-tuple-element.70), channel_id=1, source_target_pairs={{0,4},{1,5},{2,6},{3,7},{4,0},{5,1},{6,2},{7,3},{8,12},{9,13},{10,... | collective-permute-start | bytes 393224 | tf_op jit(solution)/shard_map/ppermute | solution.py:626
  40.5 6.2 %collective-permute-start.12 = (bf16[128,256]{1,0:T(8,128)(2,1)S(1)}, bf16[128,256]{1,0:T(8,128)(2,1)S(1)}, u32[]{:S(2)}, u32[]{:S(2)}) collective-permute-start(bf16[128,256]{1,0:T(8,128)(2,1)S(1)} %get-tuple-element.72), channel_id=1, source_target_pairs={{0,8},{1,9},{2,10},{3,11},{4,12},{5,13},{6,14},{7,15},{8,16},{9,17... | collective-permute-start | bytes 196616 | tf_op jit(solution)/shard_map/ppermute | solution.py:626
  41.7 6.3 %collective-permute-start.13 = (bf16[128,256]{1,0:T(8,128)(2,1)S(1)}, bf16[128,256]{1,0:T(8,128)(2,1)S(1)}, u32[]{:S(2)}, u32[]{:S(2)}) collective-permute-start(bf16[128,256]{1,0:T(8,128)(2,1)S(1)} %get-tuple-element.73), channel_id=1, source_target_pairs={{0,16},{1,17},{2,18},{3,19},{4,20},{5,21},{6,22},{7,23},{8,24},{9,... | collective-permute-start | bytes 196616 | tf_op jit(solution)/shard_map/ppermute | solution.py:626
  44.2 4.5 %collective-permute-start.14 = (bf16[128,256]{1,0:T(8,128)(2,1)S(1)}, bf16[128,256]{1,0:T(8,128)(2,1)S(1)}, u32[]{:S(2)}, u32[]{:S(2)}) collective-permute-start(bf16[128,256]{1,0:T(8,128)(2,1)S(1)} %get-tuple-element.74), channel_id=1, source_target_pairs={{0,24},{1,25},{2,26},{3,27},{4,28},{5,29},{6,30},{7,31},{8,0},{9,1... | collective-permute-start | bytes 196616 | tf_op jit(solution)/shard_map/ppermute | solution.py:626
  49.3 3.6 %collective-permute-start.16 = (f32[8,128]{1,0:T(8,128)S(1)}, f32[8,128]{1,0:T(8,128)S(1)}, u32[]{:S(2)}, u32[]{:S(2)}) collective-permute-start(f32[8,128]{1,0:T(8,128)S(1)} %get-tuple-element.76.refs_3_), channel_id=1, source_target_pairs={{0,2},{1,3},{2,0},{3,1},{4,6},{5,7},{6,4},{7,5},{8,10},{9,11},{10,... | collective-permute-start | bytes 12296 | tf_op jit(solution)/shard_map/ppermute | solution.py:626
  58.0 7.0 %collective-permute-start.19 = (bf16[48,2048]{1,0:T(8,128)(2,1)S(1)}, bf16[48,2048]{1,0:T(8,128)(2,1)S(1)}, u32[]{:S(2)}, u32[]{:S(2)}) collective-permute-start(bf16[48,2048]{1,0:T(8,128)(2,1)S(1)} %get-tuple-element.81), channel_id=1, source_target_pairs={{0,2},{1,3},{2,0},{3,1},{4,6},{5,7},{6,4},{7,5},{8,10},{9,11},{10,... | collective-permute-start | bytes 589832 | tf_op jit(solution)/shard_map/ppermute | solution.py:626
  66.4 10.6 %collective-permute-start.21 = (bf16[48,2176]{1,0:T(8,128)(2,1)S(1)}, bf16[48,2176]{1,0:T(8,128)(2,1)S(1)}, u32[]{:S(2)}, u32[]{:S(2)}) collective-permute-start(bf16[48,2176]{1,0:T(8,128)(2,1)S(1)} %collective-permute-done.20.refs_0_.s0), channel_id=1, source_target_pairs={{0,4},{1,5},{2,6},{3,7},{4,0},{5,1},{6,2},{7,3},{8,12},{9,13},{10,... | collective-permute-start | bytes 626696 | tf_op jit(solution)/shard_map/ppermute | solution.py:626
  66.9 14.7 %collective-permute-start.22 = (bf16[48,2176]{1,0:T(8,128)(2,1)S(1)}, bf16[48,2176]{1,0:T(8,128)(2,1)S(1)}, u32[]{:S(2)}, u32[]{:S(2)}) collective-permute-start(bf16[48,2176]{1,0:T(8,128)(2,1)S(1)} %collective-permute-done.20.refs_0_.s0), channel_id=1, source_target_pairs={{0,2},{1,3},{2,0},{3,1},{4,6},{5,7},{6,4},{7,5},{8,10},{9,11},{10,... | collective-permute-start | bytes 626696 | tf_op jit(solution)/shard_map/ppermute | solution.py:626
  77.1 9.2 %collective-permute-start.23 = (bf16[48,2176]{1,0:T(8,128)(2,1)S(1)}, bf16[48,2176]{1,0:T(8,128)(2,1)S(1)}, u32[]{:S(2)}, u32[]{:S(2)}) collective-permute-start(bf16[48,2176]{1,0:T(8,128)(2,1)S(1)} %collective-permute-done.20.refs_0_.s0), channel_id=1, source_target_pairs={{0,1},{1,0},{2,3},{3,2},{4,5},{5,4},{6,7},{7,6},{8,9},{9,8},{10,11... | collective-permute-start | bytes 626696 | tf_op jit(solution)/shard_map/ppermute | solution.py:626
  77.1 9.2 %collective-permute-start.24 = (bf16[48,2176]{1,0:T(8,128)(2,1)S(1)}, bf16[48,2176]{1,0:T(8,128)(2,1)S(1)}, u32[]{:S(2)}, u32[]{:S(2)}) collective-permute-start(bf16[48,2176]{1,0:T(8,128)(2,1)S(1)} %collective-permute-done.21.refs_1_), channel_id=1, source_target_pairs={{0,1},{1,0},{2,3},{3,2},{4,5},{5,4},{6,7},{7,6},{8,9},{9,8},{10,11... | collective-permute-start | bytes 626696 | tf_op jit(solution)/shard_map/ppermute | solution.py:626
  81.6 4.7 %collective-permute-start.25 = (bf16[48,2176]{1,0:T(8,128)(2,1)S(1)}, bf16[48,2176]{1,0:T(8,128)(2,1)S(1)}, u32[]{:S(2)}, u32[]{:S(2)}) collective-permute-start(bf16[48,2176]{1,0:T(8,128)(2,1)S(1)} %collective-permute-done.22.refs_2_.s1), channel_id=1, source_target_pairs={{0,1},{1,0},{2,3},{3,2},{4,5},{5,4},{6,7},{7,6},{8,9},{9,8},{10,11... | collective-permute-start | bytes 626696 | tf_op jit(solution)/shard_map/ppermute | solution.py:626
  91.7 13.9 %collective-permute-start.26 = (bf16[288,1024]{1,0:T(8,128)(2,1)S(1)}, bf16[288,1024]{1,0:T(8,128)(2,1)S(1)}, u32[]{:S(2)}, u32[]{:S(2)}) collective-permute-start(bf16[288,1024]{1,0:T(8,128)(2,1)S(1)} %get-tuple-element.87), channel_id=1, source_target_pairs={{0,1},{1,0},{2,3},{3,2},{4,5},{5,4},{6,7},{7,6},{8,9},{9,8},{10,11... | collective-permute-start | bytes 1769480 | tf_op jit(solution)/shard_map/ppermute | solution.py:626
  92.2 8.3 %collective-permute-start.29 = (bf16[48,2176]{1,0:T(8,128)(2,1)S(1)}, bf16[48,2176]{1,0:T(8,128)(2,1)S(1)}, u32[]{:S(2)}, u32[]{:S(2)}) collective-permute-start(bf16[48,2176]{1,0:T(8,128)(2,1)S(1)} %collective-permute-done.20.refs_0_.s0), channel_id=1, source_target_pairs={{0,6},{1,7},{2,4},{3,5},{4,2},{5,3},{6,0},{7,1},{8,14},{9,15},{10,... | collective-permute-start | bytes 626696 | tf_op jit(solution)/shard_map/ppermute | solution.py:626
  105.8 13.8 %collective-permute-start.27 = (bf16[192,512]{1,0:T(8,128)(2,1)S(1)}, bf16[192,512]{1,0:T(8,128)(2,1)S(1)}, u32[]{:S(2)}, u32[]{:S(2)}) collective-permute-start(bf16[192,512]{1,0:T(8,128)(2,1)S(1)} %get-tuple-element.89), channel_id=1, source_target_pairs={{0,2},{1,3},{2,0},{3,1},{4,6},{5,7},{6,4},{7,5},{8,10},{9,11},{10,... | collective-permute-start | bytes 589832 | tf_op jit(solution)/shard_map/ppermute | solution.py:626
  107.8 5.3 %collective-permute-start.32 = (bf16[96,512]{1,0:T(8,128)(2,1)S(1)}, bf16[96,512]{1,0:T(8,128)(2,1)S(1)}, u32[]{:S(2)}, u32[]{:S(2)}) collective-permute-start(bf16[96,512]{1,0:T(8,128)(2,1)S(1)} %get-tuple-element.94), channel_id=1, source_target_pairs={{0,4},{1,5},{2,6},{3,7},{4,0},{5,1},{6,2},{7,3},{8,12},{9,13},{10,... | collective-permute-start | bytes 294920 | tf_op jit(solution)/shard_map/ppermute | solution.py:626
  109.1 6.9 %collective-permute-start.33 = (bf16[96,512]{1,0:T(8,128)(2,1)S(1)}, bf16[96,512]{1,0:T(8,128)(2,1)S(1)}, u32[]{:S(2)}, u32[]{:S(2)}) collective-permute-start(bf16[96,512]{1,0:T(8,128)(2,1)S(1)} %get-tuple-element.95), channel_id=1, source_target_pairs={{0,6},{1,7},{2,4},{3,5},{4,2},{5,3},{6,0},{7,1},{8,14},{9,15},{10,... | collective-permute-start | bytes 294920 | tf_op jit(solution)/shard_map/ppermute | solution.py:626
  110.4 7.1 %collective-permute-start.28 = (bf16[96,512]{1,0:T(8,128)(2,1)S(1)}, bf16[96,512]{1,0:T(8,128)(2,1)S(1)}, u32[]{:S(2)}, u32[]{:S(2)}) collective-permute-start(bf16[96,512]{1,0:T(8,128)(2,1)S(1)} %get-tuple-element.90), channel_id=1, source_target_pairs={{0,4},{1,5},{2,6},{3,7},{4,0},{5,1},{6,2},{7,3},{8,12},{9,13},{10,... | collective-permute-start | bytes 294920 | tf_op jit(solution)/shard_map/ppermute | solution.py:626
  111.7 7.8 %collective-permute-start.34 = (bf16[96,512]{1,0:T(8,128)(2,1)S(1)}, bf16[96,512]{1,0:T(8,128)(2,1)S(1)}, u32[]{:S(2)}, u32[]{:S(2)}) collective-permute-start(bf16[96,512]{1,0:T(8,128)(2,1)S(1)} %get-tuple-element.96), channel_id=1, source_target_pairs={{0,6},{1,7},{2,4},{3,5},{4,2},{5,3},{6,0},{7,1},{8,14},{9,15},{10,... | collective-permute-start | bytes 294920 | tf_op jit(solution)/shard_map/ppermute | solution.py:626
  120.4 3.7 %collective-permute-start.36 = (f32[8,256]{1,0:T(8,128)S(1)}, f32[8,256]{1,0:T(8,128)S(1)}, u32[]{:S(2)}, u32[]{:S(2)}) collective-permute-start(f32[8,256]{1,0:T(8,128)S(1)} %get-tuple-element.98.refs_1_), channel_id=1, source_target_pairs={{0,2},{1,3},{2,0},{3,1},{4,6},{5,7},{6,4},{7,5},{8,10},{9,11},{10,... | collective-permute-start | bytes 24584 | tf_op jit(solution)/shard_map/ppermute | solution.py:626
  125.4 6.5 %collective-permute-start.38 = (bf16[48,512]{1,0:T(8,128)(2,1)S(1)}, bf16[48,512]{1,0:T(8,128)(2,1)S(1)}, u32[]{:S(2)}, u32[]{:S(2)}) collective-permute-start(bf16[48,512]{1,0:T(8,128)(2,1)S(1)} %get-tuple-element.100), channel_id=1, source_target_pairs={{0,8},{1,9},{2,10},{3,11},{4,12},{5,13},{6,14},{7,15},{8,16},{9,17... | collective-permute-start | bytes 147464 | tf_op jit(solution)/shard_map/ppermute | solution.py:626
  125.5 7.6 %collective-permute-start.39 = (bf16[48,512]{1,0:T(8,128)(2,1)S(1)}, bf16[48,512]{1,0:T(8,128)(2,1)S(1)}, u32[]{:S(2)}, u32[]{:S(2)}) collective-permute-start(bf16[48,512]{1,0:T(8,128)(2,1)S(1)} %get-tuple-element.101), channel_id=1, source_target_pairs={{0,16},{1,17},{2,18},{3,19},{4,20},{5,21},{6,22},{7,23},{8,24},{9,... | collective-permute-start | bytes 147464 | tf_op jit(solution)/shard_map/ppermute | solution.py:626
  128.2 4.9 %collective-permute-start.40 = (bf16[48,512]{1,0:T(8,128)(2,1)S(1)}, bf16[48,512]{1,0:T(8,128)(2,1)S(1)}, u32[]{:S(2)}, u32[]{:S(2)}) collective-permute-start(bf16[48,512]{1,0:T(8,128)(2,1)S(1)} %get-tuple-element.102), channel_id=1, source_target_pairs={{0,24},{1,25},{2,26},{3,27},{4,28},{5,29},{6,30},{7,31},{8,0},{9,1... | collective-permute-start | bytes 147464 | tf_op jit(solution)/shard_map/ppermute | solution.py:626
  (13 other events, 111.0 us)
where the time goes:
time: 134 us
  starting transfers between devices  55.4 us (41%)
  waiting for transfers between devices  46.2 us (34%)
  Pallas kernels  31.2 us (23%)
    ppermute x41, starting transfers between devices, move(): return lax.ppermute(v, ('sp', 'tp'), perm)  55.4 us
    ppermute x41, waiting for transfers between devices, move(): return lax.ppermute(v, ('sp', 'tp'), perm)  46.2 us
    pallas_call x15, Pallas kernels, call(): pl.pallas_call(kernel, out_shape=outs, in_specs=[local] * (len(args) - hi...  15.6 us
    pallas_call x2, Pallas kernels, experts(): pl.pallas_call(expert_kernel, grid=(hidden // chunk,), out_shape=[shape_o...  8.68 us
    pallas_call x2, Pallas kernels, load(): pl.pallas_call(lambda *refs: load_kernel(*refs[:count], *refs[count + 1:]...  6.95 us
  transfers between devices with their start and end apart: 41, of which 22 were waited for; matrix products, arithmetic and copies ran while one was open for 1% of the time, Pallas kernels for 11%

commit v1 on v0

--- a/solution.py
+++ b/solution.py
@@ -255,11 +255,10 @@
     w_out[...] = dot(m[:cap], table.astype(BF)).astype(BF)
 
 
-def pack_kernel(qa, ka, qb, kb, offs_a, offs_b, *outs):
+def pack_kernel(side, qa, ka, qb, kb, offs_a, offs_b, *outs):
     z, x, _ = spot()
     rows = qa.shape[0]
     planes = qa.shape[1] // LANE
-    same, cross = outs[:planes], outs[planes:]
 
     def offset_rows(ref, values):
         parts = []
@@ -277,22 +276,25 @@
         cols = slice(u * LANE, (u + 1) * LANE)
         kv = all_a[:, u, :].astype(BF)
         kv_beta = all_b[:, u, :].astype(BF)
-        for k in range(planes):
-
-            @pl.when(d == k)
+        for k, ref in enumerate(outs):
+
+            @pl.when((d == k) & (x == side))
             def _():
-                for flip in range(2):
-
-                    @pl.when(x == flip)
-                    def _():
-                        alpha, beta = (cross[k], same[k]) if flip else (same[k], cross[k])
-                        alpha[0:rows, 0:LANE] = qa[:, cols]
-                        alpha[0:rows, LANE : 2 * LANE] = kv
-                        offset_rows(alpha, [offs_a[2 * u : 2 * u + 1, :], offs_a[2 * u + 1 : 2 * u + 2, :]])
-                        beta[0:rows, 0:LANE] = qb[:, cols]
-                        beta[0:rows, LANE : 2 * LANE] = kv_beta[:, 0:LANE]
-                        offset_rows(beta, [offs_b[u : u + 1, :]])
-                        same[k][0:rows, 2 * LANE :] = kv_beta[:, LANE:]
+                ref[0:rows, 0:LANE] = qa[:, cols]
+                ref[0:rows, LANE : 2 * LANE] = kv
+                offset_rows(ref, [offs_a[2 * u : 2 * u + 1, :], offs_a[2 * u + 1 : 2 * u + 2, :]])
+
+            @pl.when((d == k) & (x != side))
+            def _():
+                ref[0:rows, 0:LANE] = qb[:, cols]
+                ref[0:rows, LANE : 2 * LANE] = kv_beta[:, 0:LANE]
+                offset_rows(ref, [offs_b[u : u + 1, :]])
+
+            if side == 0:
+
+                @pl.when(d == k)
+                def _():
+                    ref[0:rows, 2 * LANE :] = kv_beta[:, LANE:]
 
 
 def relay_kernel(*refs):
@@ -326,7 +328,7 @@
                 off_s[h : h + 1, at] = LOG2E * jnp.sum(lines[3 * h : 3 * h + 3], axis=0, keepdims=True)
 
 
-def attend_half(planes, side, q_s, k_s, v_s, off_s, out, acc_s, rest_s, tri_s):
+def attend_half(planes, side, q_s, k_s, v_s, off_s, out, acc_s, tri_s):
     z, x, _ = spot()
     rows = k_s.shape[0] // (2 * planes)
     tile = 2 * rows
@@ -338,38 +340,67 @@
     scale = jnp.where(x == 0, (LANE // 2) ** (-0.5) * LOG2E, LANE ** (-0.5) * LOG2E).astype(F32)
     base = side * (planes * rows)
 
-    def one_head(h, carry):
+    def run(heads):
+        tasks = []
         for j in range(planes - 1, -1, -1):
+            for first in range(j, planes, 2):
+                tasks += [(h, j, first, min(2, planes - first)) for h in range(heads)]
+        rest = {}
+
+        def product(task):
+            h, j, first, count = task
             cols = slice(j * tile, (j + 1) * tile)
-            first = j * rows
-            while first < planes * rows:
-                count = min(tile, planes * rows - first)
-                at = slice(first, first + count)
-                diagonal = first == j * rows
-                fresh = rows if diagonal else 0
-                q = q_s[h, pl.ds(pl.multiple_of(base + first, rows), count), :]
-                s = dot(q, k_s[cols, :], ((1,), (1,))) * scale + off_s[pl.ds(h, 1), cols]
-                top = jnp.minimum(s, 64.0)
-                take = top - jnp.log2(1.0 + jnp.exp2(top))
-                soft = s - take
-                if diagonal:
-                    soft = jnp.where(valid[:count], soft, 0.0)
-                soft = soft.astype(BF)
-                after = dot(soft, tri_s[...])
-                if fresh:
-                    rest_s[first : first + rows, :] = jnp.zeros((rows, 1), F32)
-                    acc_s[h, first : first + rows, :] = jnp.zeros((rows, LANE), F32)
-                rest = rest_s[at, :]
-                w = jnp.exp2(take - (after + rest))
-                if diagonal:
-                    w = jnp.where(valid[:count], w, 0.0)
-                acc_s[h, at, :] = acc_s[h, at, :] + dot(w.astype(BF), v_s[cols, :])
-                if j > 0:
-                    rest_s[at, :] = rest + after[:, 0:1] + soft[:, 0:1].astype(F32)
-                first += count
-        return carry
-
-    lax.fori_loop(0, jnp.where(x == 0, 2, 1), one_head, 0)
+            at = pl.ds(pl.multiple_of(base + first * rows, rows), count * rows)
+            return dot(q_s[h, at, :], k_s[cols, :], ((1,), (1,)))
+
+        def suffix(task, s):
+            h, j, first, count = task
+            s = s * scale + off_s[h : h + 1, j * tile : (j + 1) * tile]
+            top = jnp.minimum(s, 64.0)
+            take = top - jnp.log2(1.0 + jnp.exp2(top))
+            soft = s - take
+            if first == j:
+                soft = jnp.where(valid[: count * rows], soft, 0.0)
+            soft = soft.astype(BF)
+            after = dot(soft, tri_s[...])
+            return take, after, soft[:, 0:1].astype(F32)
+
+        def gather(task, take, after, own):
+            h, j, first, count = task
+            fresh = first == j
+            blocks = range(first, first + count)
+            zero = jnp.zeros((rows, 1), F32)
+            before = [rest.get((h, i), zero) for i in blocks]
+            before = before[0] if count == 1 else jnp.concatenate(before, axis=0)
+            w = jnp.exp2(take - (after + before))
+            if fresh:
+                w = jnp.where(valid[: count * rows], w, 0.0)
+            part = dot(w.astype(BF), v_s[j * tile : (j + 1) * tile, :])
+            total = before + after[:, 0:1] + own
+            for k, i in enumerate(blocks):
+                at = slice(i * rows, (i + 1) * rows)
+                piece = part[k * rows : (k + 1) * rows]
+                acc_s[h, at, :] = piece if i == j else acc_s[h, at, :] + piece
+                rest[(h, i)] = total[k * rows : (k + 1) * rows]
+
+        count = len(tasks)
+        ahead, middle = {}, {}
+        for n in range(count + 2):
+            if n < count:
+                ahead[n] = product(tasks[n])
+            if 0 <= n - 1 < count:
+                middle[n - 1] = suffix(tasks[n - 1], ahead.pop(n - 1))
+            if 0 <= n - 2:
+                gather(tasks[n - 2], *middle.pop(n - 2))
+
+    @pl.when(x == 0)
+    def _():
+        run(2)
+
+    @pl.when(x != 0)
+    def _():
+        run(1)
+
     for d in range(planes):
         at = pl.ds(pl.multiple_of(((z + d) % planes) * rows, rows), rows)
         value = jnp.where(low | (x != 0), acc_s[0, at, :], acc_s[1, at, :])
@@ -471,43 +502,44 @@
 
 
 def expert_kernel(*refs):
-    gate, up, down, near, far, x_s, acc_s, w_s = refs[-8:]
-    count = x_s.shape[0] // refs[0].shape[0]
-    pieces = refs[:count]
-    step = pl.program_id(0)
-    n = pieces[0].shape[0]
+    gate, up, down, near, far, x_s, h_s, w_s = refs[-8:]
+    n = refs[0].shape[0]
+    count = x_s.shape[0] // n
     columns = x_s.shape[1]
-
-    @pl.when(step == 0)
-    def _():
-        odd = lax.axis_index("sp") % 2 != 0
-        for k in range(count):
-            at = slice(k * n, (k + 1) * n)
-            x_s[at, :] = pieces[k][:, 0:columns]
-            w = pieces[k][:, columns : columns + LANE].astype(F32)
-            even_w = w[:, 0:1] + w[:, 1:2] + w[:, 2:3]
-            odd_w = w[:, 3:4] + w[:, 4:5] + w[:, 5:6]
-            w_s[at, :] = jnp.where(odd, odd_w, even_w)
-        acc_s[...] = jnp.zeros_like(acc_s)
+    odd = lax.axis_index("sp") % 2 != 0
+    _, _, t = spot()
+    for k, piece in enumerate(refs[:count]):
+        at = slice(k * n, (k + 1) * n)
+        x_s[at, :] = piece[:, 0:columns]
+        w = piece[:, columns : columns + LANE].astype(F32)
+        even_w = w[:, 0:1] + w[:, 1:2] + w[:, 2:3]
+        odd_w = w[:, 3:4] + w[:, 4:5] + w[:, 5:6]
+        w_s[at, :] = jnp.where(odd, odd_w, even_w)
 
     x = x_s[...]
-    g = dot(x, gate[0])
-    u = dot(x, up[0])
-    hidden = (g / (1.0 + jnp.exp(-g)) * u).astype(BF)
-    acc_s[...] += dot(hidden, down[0])
-
-    @pl.when(step == pl.num_programs(0) - 1)
-    def _():
-        mid = count // 2 * n
-        width = near.shape[1] // 2
-        _, _, t = spot()
-        for k in range(2):
-            cols = slice(k * width, (k + 1) * width)
-            at = pl.ds(pl.multiple_of((t ^ (2 * k)) * width, LANE), width)
-            near[:, cols] = (acc_s[:, at] * w_s[...]).astype(BF)
-            at = pl.ds(pl.multiple_of((t ^ (2 * k + 1)) * width, LANE), width)
-            far[0:mid, cols] = (acc_s[mid:, at] * w_s[mid:, :]).astype(BF)
-            far[mid:, cols] = (acc_s[0:mid, at] * w_s[0:mid, :]).astype(BF)
+    chunk = 2 * LANE
+    chunks = h_s.shape[1] // chunk
+    ahead = None
+    for k in range(chunks + 1):
+        this = None
+        if k < chunks:
+            at = slice(k * chunk, (k + 1) * chunk)
+            this = dot(x, gate[0, :, at]), dot(x, up[0, :, at])
+        if ahead is not None:
+            g, u = ahead
+            h_s[:, (k - 1) * chunk : k * chunk] = (g / (1.0 + jnp.exp(-g)) * u).astype(BF)
+        ahead = this
+
+    mid = count // 2 * n
+    width = near.shape[1] // 2
+    for k in range(2):
+        cols = slice(k * width, (k + 1) * width)
+        at = pl.ds(pl.multiple_of((t ^ (2 * k + 1)) * width, LANE), width)
+        value = (dot(h_s[...], down[0, :, at]) * w_s[...]).astype(BF)
+        far[0:mid, cols] = value[mid:]
+        far[mid:, cols] = value[:mid]
+        at = pl.ds(pl.multiple_of((t ^ (2 * k)) * width, LANE), width)
+        near[:, cols] = (dot(h_s[...], down[0, :, at]) * w_s[...]).astype(BF)
 
 
 def chip_kernel(spots, targets, near, got, *refs):
@@ -632,26 +664,28 @@
         return move(v, lambda z, x, t: (z, x, t ^ k))
 
     def across_tp(v):
-        other_y = swap_tp(v, 2)
-        return v, swap_tp(v, 1), other_y, swap_tp(other_y, 1)
+        return v, swap_tp(v, 1), swap_tp(v, 2), swap_tp(v, 3)
 
     def swap_plane(v, dx, k):
         return move(v, lambda z, x, t: (z, x ^ dx, t ^ k))
 
-    packed = call(
-        pack_kernel,
-        [shape_of((rows + 8, 3 * LANE))] * planes + [shape_of((rows + 8, 2 * LANE))] * planes,
-        in_hbm(
-            query_alpha,
-            pairs_alpha,
-            query_beta,
-            pairs_beta,
-            jnp.transpose(offset_alpha),
-            jnp.transpose(offset_beta),
-        ),
-        12,
-    )
-    same, cross = packed[:planes], packed[planes:]
+    inputs = in_hbm(
+        query_alpha,
+        pairs_alpha,
+        query_beta,
+        pairs_beta,
+        jnp.transpose(offset_alpha),
+        jnp.transpose(offset_beta),
+    )
+    same, cross = (
+        call(
+            lambda *refs: pack_kernel(flip, *refs),
+            [shape_of((rows + 8, (3 - flip) * LANE))] * planes,
+            inputs,
+            12,
+        )
+        for flip in range(2)
+    )
     got_same, got_cross = [same[0]] + [None] * (planes - 1), [None] * planes
     for d in (2, 1, 3):
         got_same[d] = shift(same[d], d, 0)
@@ -688,7 +722,6 @@
     spare = (m, n, w, *lines[1:], p_alpha)
     work = [
         pltpu.VMEM((2, planes * rows, LANE), F32),
-        pltpu.VMEM((planes * rows, 1), F32),
         pltpu.VMEM((2 * rows, 2 * rows), BF),
     ]
     half = shape_of((planes * rows, LANE))
@@ -742,37 +775,25 @@
         return g, x, 2 * (t >> 1) + (z >> 1)
 
     mine = move(settled, to_plane)
-    from_x, from_y, from_xy = (
-        swap_plane(mine, 1, 0),
-        swap_plane(mine, 0, 2),
-        swap_plane(mine, 1, 2),
-    )
+    from_x, from_y = swap_plane(mine, 1, 0), swap_plane(mine, 0, 2)
+    from_xy = swap_plane(from_x, 0, 2)
     near = [mine, from_x, from_y]
     far = [swap_plane(mine, 0, 1)] + [swap_plane(v, 0, 1) for v in near[1:]]
     hidden = expert_gate.shape[2]
-    chunk = hidden // 2
 
     def experts(pieces):
         n = len(pieces) * cap
-        out = pl.BlockSpec((n, 2 * width), lambda j: (0, 0))
-        return pl.pallas_call(
+        return call(
             expert_kernel,
-            grid=(hidden // chunk,),
-            out_shape=[shape_of((n, 2 * width))] * 2,
-            in_specs=[pl.BlockSpec((cap, columns + LANE), lambda j: (0, 0))] * len(pieces)
-            + [
-                pl.BlockSpec((1, columns, chunk), lambda j: (0, 0, j)),
-                pl.BlockSpec((1, columns, chunk), lambda j: (0, 0, j)),
-                pl.BlockSpec((1, chunk, columns), lambda j: (0, j, 0)),
-            ],
-            out_specs=[out] * 2,
-            scratch_shapes=[
+            [shape_of((n, 2 * width))] * 2,
+            (*pieces, e_gate, e_up, e_down),
+            24,
+            scratch=[
                 pltpu.VMEM((n, columns), BF),
-                pltpu.VMEM((n, columns), F32),
+                pltpu.VMEM((n, hidden), BF),
                 pltpu.VMEM((n, 1), F32),
             ],
-            compiler_params=pltpu.CompilerParams(vmem_limit_bytes=24 << 20),
-        )(*pieces, e_gate, e_up, e_down)
+        )
 
     def chip(spots, targets, outs, own, got):
         kernel = lambda *refs: chip_kernel(spots, targets, *refs)

time: 134 us -> 129 us (0.963)
  Pallas kernels: 31.2 us -> 28.1 us
  waiting for transfers between devices: 46.2 us -> 44.6 us
    pallas_call x2 -> x0, Pallas kernels: 8.68 us -> none  [experts(): pl.pallas_call(expert_kernel, grid=(hidden // chunk,), out_shape=[shape_o...]
    pallas_call x15 -> x18, Pallas kernels: 15.6 us -> 21.1 us  [call(): pl.pallas_call(kernel, out_shape=outs, in_specs=[local] * (len(args) - hi...]
    ppermute x41, waiting for transfers between devices: 46.2 us -> 44.6 us  [move(): return lax.ppermute(v, ('sp', 'tp'), perm)]
  transfers between devices with their start and end apart: 41 -> 41, of which waited for: 22 -> 21; matrix products, arithmetic and copies ran while one was open for 1% -> 1% of each run, Pallas kernels for 11% -> 11%
where the time goes in v1:
time: 129 us
  starting transfers between devices  55.4 us (43%)
  waiting for transfers between devices  44.6 us (35%)
  Pallas kernels  28.1 us (22%)
    ppermute x41, starting transfers between devices, move(): return lax.ppermute(v, ('sp', 'tp'), perm)  55.4 us
    ppermute x41, waiting for transfers between devices, move(): return lax.ppermute(v, ('sp', 'tp'), perm)  44.6 us
    pallas_call x18, Pallas kernels, call(): pl.pallas_call(kernel, out_shape=outs, in_specs=[local] * (len(args) - hi...  21.1 us
    pallas_call x2, Pallas kernels, load(): pl.pallas_call(lambda *refs: load_kernel(*refs[:count], *refs[count + 1:]...  6.95 us
  transfers between devices with their start and end apart: 41, of which 21 were waited for; matrix products, arithmetic and copies ran while one was open for 1% of the time, Pallas kernels for 11%

profile of v1, /device:TPU:0, one launch (start us, length us, event | category | flops | bytes accessed | tf_op | source)
XLA Modules:
  0.0 129.1 jit_solution(3925724837574494016)
XLA Ops:
  0.0 2.3 %shard_map.190 = (bf16[136,384]{1,0:T(8,128)(2,1)S(1)}, bf16[136,384]{1,0:T(8,128)(2,1)S(1)}, bf16[136,384]{1,0:T(8,128)(2,1)S(1)}, bf16[136,384]{1,0:T(8,128)(2,1)S(1)}) custom-call(bf16[128,512]{1,0:T(8,128)(2,1)} %refs_0_.5, bf16[128,4,128]{2,1,0:T(4,128)(2,1)} %refs_1_.5, bf16[128,512]{1,0:T(8,128)(2,1)} %refs_2_.5, bf16[128,4,256]{2,1,0:T(4,128)(2,1)} %refs_3_.3, ...), custom_call_target="tpu_custom_call" | custom-call | tf_op jit(solution)/shard_map/pallas_call | solution.py:203
  2.3 4.1 %collective-permute-start = (bf16[136,384]{1,0:T(8,128)(2,1)S(1)}, bf16[136,384]{1,0:T(8,128)(2,1)S(1)}, u32[]{:S(2)}, u32[]{:S(2)}) collective-permute-start(bf16[136,384]{1,0:T(8,128)(2,1)S(1)} %get-tuple-element.54), channel_id=1, source_target_pairs={{0,16},{1,17},{2,18},{3,19},{4,20},{5,21},{6,22},{7,23},{8,24},{9,... | collective-permute-start | bytes 313352 | tf_op jit(solution)/shard_map/ppermute | solution.py:658
  8.0 2.2 %collective-permute-start.2 = (bf16[136,384]{1,0:T(8,128)(2,1)S(1)}, bf16[136,384]{1,0:T(8,128)(2,1)S(1)}, u32[]{:S(2)}, u32[]{:S(2)}) collective-permute-start(bf16[136,384]{1,0:T(8,128)(2,1)S(1)} %get-tuple-element.58), channel_id=1, source_target_pairs={{0,24},{1,25},{2,26},{3,27},{4,28},{5,29},{6,30},{7,31},{8,0},{9,1... | collective-permute-start | bytes 313352 | tf_op jit(solution)/shard_map/ppermute | solution.py:658
  10.2 4.5 %collective-permute-done.refs_2_ = bf16[136,384]{1,0:T(8,128)(2,1)S(1)} collective-permute-done((bf16[136,384]{1,0:T(8,128)(2,1)S(1)}, bf16[136,384]{1,0:T(8,128)(2,1)S(1)}, u32[]{:S(2)}, u32[]{:S(2)}) %collective-permute-start) | collective-permute-done | bytes 104480 | tf_op jit(solution)/shard_map/ppermute | solution.py:658
  15.4 1.6 %collective-permute-start.7 = (bf16[512,128]{1,0:T(8,128)(2,1)S(1)}, bf16[512,128]{1,0:T(8,128)(2,1)S(1)}, u32[]{:S(2)}, u32[]{:S(2)}) collective-permute-start(bf16[512,128]{1,0:T(8,128)(2,1)S(1)} %shard_map.193), channel_id=1, source_target_pairs={{0,4},{1,5},{2,6},{3,7},{4,0},{5,1},{6,2},{7,3},{8,12},{9,13},{10,... | collective-permute-start | bytes 393224 | tf_op jit(solution)/shard_map/ppermute | solution.py:658
  17.8 1.6 %collective-permute-start.8 = (f32[2,512]{1,0:T(2,128)S(1)}, f32[2,512]{1,0:T(2,128)S(1)}, u32[]{:S(2)}, u32[]{:S(2)}) collective-permute-start(f32[2,512]{1,0:T(2,128)S(1)} %pad_maximum_fusion.l0), channel_id=1, source_target_pairs={{0,1},{1,0},{2,3},{3,2},{4,5},{5,4},{6,7},{7,6},{8,9},{9,8},{10,11... | collective-permute-start | bytes 12296 | tf_op jit(solution)/shard_map/ppermute | solution.py:658
  19.9 1.8 %shard_map.192 = (bf16[136,256]{1,0:T(8,128)(2,1)S(1)}, bf16[136,256]{1,0:T(8,128)(2,1)S(1)}, bf16[136,256]{1,0:T(8,128)(2,1)S(1)}, bf16[136,256]{1,0:T(8,128)(2,1)S(1)}) custom-call(bf16[128,512]{1,0:T(8,128)(2,1)} %refs_0_.5, bf16[128,4,128]{2,1,0:T(4,128)(2,1)} %refs_1_.5, bf16[128,512]{1,0:T(8,128)(2,1)} %refs_2_.5, bf16[128,4,256]{2,1,0:T(4,128)(2,1)} %refs_3_.3, ...), custom_call_target="tpu_custom_call" | custom-call | tf_op jit(solution)/shard_map/pallas_call | solution.py:203
  22.3 2.3 %collective-permute-start.4 = (bf16[136,256]{1,0:T(8,128)(2,1)S(1)}, bf16[136,256]{1,0:T(8,128)(2,1)S(1)}, u32[]{:S(2)}, u32[]{:S(2)}) collective-permute-start(bf16[136,256]{1,0:T(8,128)(2,1)S(1)} %get-tuple-element.60), channel_id=1, source_target_pairs={{0,12},{1,13},{2,14},{3,15},{4,8},{5,9},{6,10},{7,11},{8,20},{9,21... | collective-permute-start | bytes 208904 | tf_op jit(solution)/shard_map/ppermute | solution.py:658
  24.6 2.0 %collective-permute-start.5 = (bf16[136,256]{1,0:T(8,128)(2,1)S(1)}, bf16[136,256]{1,0:T(8,128)(2,1)S(1)}, u32[]{:S(2)}, u32[]{:S(2)}) collective-permute-start(bf16[136,256]{1,0:T(8,128)(2,1)S(1)} %get-tuple-element.61), channel_id=1, source_target_pairs={{0,20},{1,21},{2,22},{3,23},{4,16},{5,17},{6,18},{7,19},{8,28},{9,... | collective-permute-start | bytes 208904 | tf_op jit(solution)/shard_map/ppermute | solution.py:658
  26.6 3.8 %collective-permute-start.6 = (bf16[136,256]{1,0:T(8,128)(2,1)S(1)}, bf16[136,256]{1,0:T(8,128)(2,1)S(1)}, u32[]{:S(2)}, u32[]{:S(2)}) collective-permute-start(bf16[136,256]{1,0:T(8,128)(2,1)S(1)} %get-tuple-element.62), channel_id=1, source_target_pairs={{0,28},{1,29},{2,30},{3,31},{4,24},{5,25},{6,26},{7,27},{8,4},{9,5... | collective-permute-start | bytes 208904 | tf_op jit(solution)/shard_map/ppermute | solution.py:658
  31.3 2.3 %shard_map.194 = (bf16[512,2048]{1,0:T(8,128)(2,1)S(1)}, bf16[512,2048]{1,0:T(8,128)(2,1)S(1)}) custom-call(bf16[512,2048]{1,0:T(8,128)(2,1)} %refs_0_.6, bf16[512,2048]{1,0:T(8,128)(2,1)} %refs_1_.6, bf16[136,384]{1,0:T(8,128)(2,1)S(1)} %collective-permute-done.refs_2_), custom_call_target="tpu_custom_call" | custom-call | tf_op jit(solution)/shard_map/pallas_call | solution.py:710
  33.6 2.2 %shard_map.195 = (bf16[512,128]{1,0:T(8,128)(2,1)S(1)}, bf16[2,1024,128]{2,1,0:T(8,128)(2,1)S(1)}, bf16[1024,128]{1,0:T(8,128)(2,1)S(1)}, bf16[1024,128]{1,0:T(8,128)(2,1)S(1)}, f32[8,1024]{1,0:T(8,128)S(1)}) custom-call(bf16[136,384]{1,0:T(8,128)(2,1)S(1)} %get-tuple-element.56.refs_0_, bf16[136,384]{1,0:T(8,128)(2,1)S(1)} %collective-permute-done.1.refs_1_, ...), custom_call_target="tpu_custom_call" | custom-call | tf_op jit(solution)/shard_map/pallas_call | solution.py:203
  36.0 2.1 %shard_map.196.own = bf16[512,128]{1,0:T(8,128)(2,1)S(1)} custom-call(bf16[2,1024,128]{2,1,0:T(8,128)(2,1)S(1)} %get-tuple-element.66.refs_0_, bf16[1024,128]{1,0:T(8,128)(2,1)S(1)} %get-tuple-element.67.refs_1_, bf16[1024,128]{1,0:T(8,128)(2,1)S(1)} %get-tuple-element.68.refs_2_, f32[8,1024]{1,0:T(8,128)S(1)} %get-tuple-element.69.refs_3_), custom_call_target="tpu_custom_call" | custom-call | tf_op jit(solution)/shard_map/pallas_call | solution.py:203
  38.1 2.8 %collective-permute-done.11.got = bf16[512,128]{1,0:T(8,128)(2,1)S(1)} collective-permute-done((bf16[512,128]{1,0:T(8,128)(2,1)S(1)}, bf16[512,128]{1,0:T(8,128)(2,1)S(1)}, u32[]{:S(2)}, u32[]{:S(2)}) %collective-permute-start.11) | collective-permute-done | bytes 131104 | tf_op jit(solution)/shard_map/ppermute | solution.py:658
  41.3 3.1 %collective-permute-start.13 = (bf16[128,256]{1,0:T(8,128)(2,1)S(1)}, bf16[128,256]{1,0:T(8,128)(2,1)S(1)}, u32[]{:S(2)}, u32[]{:S(2)}) collective-permute-start(bf16[128,256]{1,0:T(8,128)(2,1)S(1)} %get-tuple-element.73), channel_id=1, source_target_pairs={{0,16},{1,17},{2,18},{3,19},{4,20},{5,21},{6,22},{7,23},{8,24},{9,... | collective-permute-start | bytes 196616 | tf_op jit(solution)/shard_map/ppermute | solution.py:658
  44.9 2.3 %collective-permute-done.12.refs_1_ = bf16[128,256]{1,0:T(8,128)(2,1)S(1)} collective-permute-done((bf16[128,256]{1,0:T(8,128)(2,1)S(1)}, bf16[128,256]{1,0:T(8,128)(2,1)S(1)}, u32[]{:S(2)}, u32[]{:S(2)}) %collective-permute-start.12) | collective-permute-done | bytes 65568 | tf_op jit(solution)/shard_map/ppermute | solution.py:658
  51.2 1.8 %collective-permute-done.16.refs_5_ = f32[8,128]{1,0:T(8,128)S(1)} collective-permute-done((f32[8,128]{1,0:T(8,128)S(1)}, f32[8,128]{1,0:T(8,128)S(1)}, u32[]{:S(2)}, u32[]{:S(2)}) %collective-permute-start.16) | collective-permute-done | bytes 4128 | tf_op jit(solution)/shard_map/ppermute | solution.py:658
  53.9 2.1 %shard_map.199 = (bf16[96,2048]{1,0:T(8,128)(2,1)S(1)}, bf16[96,2048]{1,0:T(8,128)(2,1)S(1)}) custom-call(bf16[128,1024]{1,0:T(8,128)(2,1)S(1)} %get-tuple-element.75.refs_0_, bf16[192,128]{1,0:T(8,128)(2,1)S(1)} %get-tuple-element.63.refs_9_.refs_1_, bf16[128,512]{1,0:T(8,128)(2,1)} %refs_2_.6, f32[8,128]{1,0:T(8,128)S(1)} %get-tuple-element.76.refs_3_, ...), custom_call_target="tpu_custom_call" | custom-call | tf_op jit(solution)/shard_map/pallas_call | solution.py:203
  58.5 6.4 %collective-permute-done.19.got = bf16[48,2048]{1,0:T(8,128)(2,1)S(1)} collective-permute-done((bf16[48,2048]{1,0:T(8,128)(2,1)S(1)}, bf16[48,2048]{1,0:T(8,128)(2,1)S(1)}, u32[]{:S(2)}, u32[]{:S(2)}) %collective-permute-start.19) | collective-permute-done | bytes 196640 | tf_op jit(solution)/shard_map/ppermute | solution.py:658
  67.0 9.7 %collective-permute-start.22 = (bf16[48,2176]{1,0:T(8,128)(2,1)S(1)}, bf16[48,2176]{1,0:T(8,128)(2,1)S(1)}, u32[]{:S(2)}, u32[]{:S(2)}) collective-permute-start(bf16[48,2176]{1,0:T(8,128)(2,1)S(1)} %collective-permute-done.20.refs_0_.s0), channel_id=1, source_target_pairs={{0,2},{1,3},{2,0},{3,1},{4,6},{5,7},{6,4},{7,5},{8,10},{9,11},{10,... | collective-permute-start | bytes 626696 | tf_op jit(solution)/shard_map/ppermute | solution.py:658
  76.7 2.4 %collective-permute-start.24 = (bf16[48,2176]{1,0:T(8,128)(2,1)S(1)}, bf16[48,2176]{1,0:T(8,128)(2,1)S(1)}, u32[]{:S(2)}, u32[]{:S(2)}) collective-permute-start(bf16[48,2176]{1,0:T(8,128)(2,1)S(1)} %collective-permute-done.21.refs_1_), channel_id=1, source_target_pairs={{0,1},{1,0},{2,3},{3,2},{4,5},{5,4},{6,7},{7,6},{8,9},{9,8},{10,11... | collective-permute-start | bytes 626696 | tf_op jit(solution)/shard_map/ppermute | solution.py:658
  79.1 2.1 %collective-permute-done.22.refs_2_.s1 = bf16[48,2176]{1,0:T(8,128)(2,1)S(1)} collective-permute-done((bf16[48,2176]{1,0:T(8,128)(2,1)S(1)}, bf16[48,2176]{1,0:T(8,128)(2,1)S(1)}, u32[]{:S(2)}, u32[]{:S(2)}) %collective-permute-start.22) | collective-permute-done | bytes 208928 | tf_op jit(solution)/shard_map/ppermute | solution.py:658
  81.2 4.7 %shard_map.202 = (bf16[1,2048,1024]{2,1,0:T(8,128)(2,1)S(1)}, bf16[1,2048,1024]{2,1,0:T(8,128)(2,1)S(1)}, bf16[1,1024,2048]{2,1,0:T(8,128)(2,1)S(1)}) custom-call(bf16[1,2048,1024]{2,1,0:T(8,128)(2,1)} %refs_0_.7, bf16[1,2048,1024]{2,1,0:T(8,128)(2,1)} %refs_1_.7, bf16[1,1024,2048]{2,1,0:T(8,128)(2,1)} %refs_2_.7, ...), custom_call_target="tpu_custom_call" | custom-call | tf_op jit(solution)/shard_map/pallas_call | solution.py:710
  85.9 4.0 %shard_map.203 = (bf16[288,1024]{1,0:T(8,128)(2,1)S(1)}, bf16[288,1024]{1,0:T(8,128)(2,1)S(1)}) custom-call(bf16[48,2176]{1,0:T(8,128)(2,1)S(1)} %collective-permute-done.20.refs_0_.s0, bf16[48,2176]{1,0:T(8,128)(2,1)S(1)} %collective-permute-done.21.refs_1_, bf16[48,2176]{1,0:T(8,128)(2,1)S(1)} %collective-permute-done.22.refs_2_.s1, ...), custom_call_target="tpu_custom_call" | custom-call | tf_op jit(solution)/shard_map/pallas_call | solution.py:203
  92.0 5.8 %collective-permute-done.29.refs_0_ = bf16[48,2176]{1,0:T(8,128)(2,1)S(1)} collective-permute-done((bf16[48,2176]{1,0:T(8,128)(2,1)S(1)}, bf16[48,2176]{1,0:T(8,128)(2,1)S(1)}, u32[]{:S(2)}, u32[]{:S(2)}) %collective-permute-start.29) | collective-permute-done | bytes 208928 | tf_op jit(solution)/shard_map/ppermute | solution.py:658
  99.3 2.2 %shard_map.205 = (bf16[96,1024]{1,0:T(8,128)(2,1)S(1)}, bf16[96,1024]{1,0:T(8,128)(2,1)S(1)}) custom-call(bf16[48,2176]{1,0:T(8,128)(2,1)S(1)} %collective-permute-done.29.refs_0_, bf16[48,2176]{1,0:T(8,128)(2,1)S(1)} %collective-permute-done.30.refs_1_, bf16[1,2048,1024]{2,1,0:T(8,128)(2,1)S(1)} %get-tuple-element.83.refs_6_.refs_2_, ...), custom_call_target="tpu_custom_call" | custom-call | tf_op jit(solution)/shard_map/pallas_call | solution.py:203
  101.8 1.8 %collective-permute-start.27 = (bf16[192,512]{1,0:T(8,128)(2,1)S(1)}, bf16[192,512]{1,0:T(8,128)(2,1)S(1)}, u32[]{:S(2)}, u32[]{:S(2)}) collective-permute-start(bf16[192,512]{1,0:T(8,128)(2,1)S(1)} %get-tuple-element.89), channel_id=1, source_target_pairs={{0,2},{1,3},{2,0},{3,1},{4,6},{5,7},{6,4},{7,5},{8,10},{9,11},{10,... | collective-permute-start | bytes 589832 | tf_op jit(solution)/shard_map/ppermute | solution.py:658
  109.0 3.0 %collective-permute-done.33.gxy0 = bf16[96,512]{1,0:T(8,128)(2,1)S(1)} collective-permute-done((bf16[96,512]{1,0:T(8,128)(2,1)S(1)}, bf16[96,512]{1,0:T(8,128)(2,1)S(1)}, u32[]{:S(2)}, u32[]{:S(2)}) %collective-permute-start.33) | collective-permute-done | bytes 98336 | tf_op jit(solution)/shard_map/ppermute | solution.py:658
  113.4 2.0 %collective-permute-done.34.gxy1 = bf16[96,512]{1,0:T(8,128)(2,1)S(1)} collective-permute-done((bf16[96,512]{1,0:T(8,128)(2,1)S(1)}, bf16[96,512]{1,0:T(8,128)(2,1)S(1)}, u32[]{:S(2)}, u32[]{:S(2)}) %collective-permute-start.34) | collective-permute-done | bytes 98336 | tf_op jit(solution)/shard_map/ppermute | solution.py:658
  118.2 1.8 %collective-permute-done.36.refs_3_ = f32[8,256]{1,0:T(8,128)S(1)} collective-permute-done((f32[8,256]{1,0:T(8,128)S(1)}, f32[8,256]{1,0:T(8,128)S(1)}, u32[]{:S(2)}, u32[]{:S(2)}) %collective-permute-start.36) | collective-permute-done | bytes 8224 | tf_op jit(solution)/shard_map/ppermute | solution.py:658
  120.8 2.5 %collective-permute-start.39 = (bf16[48,512]{1,0:T(8,128)(2,1)S(1)}, bf16[48,512]{1,0:T(8,128)(2,1)S(1)}, u32[]{:S(2)}, u32[]{:S(2)}) collective-permute-start(bf16[48,512]{1,0:T(8,128)(2,1)S(1)} %get-tuple-element.101), channel_id=1, source_target_pairs={{0,16},{1,17},{2,18},{3,19},{4,20},{5,21},{6,22},{7,23},{8,24},{9,... | collective-permute-start | bytes 147464 | tf_op jit(solution)/shard_map/ppermute | solution.py:658
  124.4 2.6 %collective-permute-done.38.f1 = bf16[48,512]{1,0:T(8,128)(2,1)S(1)} collective-permute-done((bf16[48,512]{1,0:T(8,128)(2,1)S(1)}, bf16[48,512]{1,0:T(8,128)(2,1)S(1)}, u32[]{:S(2)}, u32[]{:S(2)}) %collective-permute-start.38) | collective-permute-done | bytes 49184 | tf_op jit(solution)/shard_map/ppermute | solution.py:658
  (81 shorter events, 33.0 us)
Async XLA Ops:
  2.3 12.4 %collective-permute-start = (bf16[136,384]{1,0:T(8,128)(2,1)S(1)}, bf16[136,384]{1,0:T(8,128)(2,1)S(1)}, u32[]{:S(2)}, u32[]{:S(2)}) collective-permute-start(bf16[136,384]{1,0:T(8,128)(2,1)S(1)} %get-tuple-element.54), channel_id=1, source_target_pairs={{0,16},{1,17},{2,18},{3,19},{4,20},{5,21},{6,22},{7,23},{8,24},{9,... | collective-permute-start | bytes 313352 | tf_op jit(solution)/shard_map/ppermute | solution.py:658
  6.4 8.3 %collective-permute-start.1 = (bf16[136,384]{1,0:T(8,128)(2,1)S(1)}, bf16[136,384]{1,0:T(8,128)(2,1)S(1)}, u32[]{:S(2)}, u32[]{:S(2)}) collective-permute-start(bf16[136,384]{1,0:T(8,128)(2,1)S(1)} %get-tuple-element.57), channel_id=1, source_target_pairs={{0,8},{1,9},{2,10},{3,11},{4,12},{5,13},{6,14},{7,15},{8,16},{9,17... | collective-permute-start | bytes 313352 | tf_op jit(solution)/shard_map/ppermute | solution.py:658
  8.0 7.4 %collective-permute-start.2 = (bf16[136,384]{1,0:T(8,128)(2,1)S(1)}, bf16[136,384]{1,0:T(8,128)(2,1)S(1)}, u32[]{:S(2)}, u32[]{:S(2)}) collective-permute-start(bf16[136,384]{1,0:T(8,128)(2,1)S(1)} %get-tuple-element.58), channel_id=1, source_target_pairs={{0,24},{1,25},{2,26},{3,27},{4,28},{5,29},{6,30},{7,31},{8,0},{9,1... | collective-permute-start | bytes 313352 | tf_op jit(solution)/shard_map/ppermute | solution.py:658
  15.4 18.2 %collective-permute-start.7 = (bf16[512,128]{1,0:T(8,128)(2,1)S(1)}, bf16[512,128]{1,0:T(8,128)(2,1)S(1)}, u32[]{:S(2)}, u32[]{:S(2)}) collective-permute-start(bf16[512,128]{1,0:T(8,128)(2,1)S(1)} %shard_map.193), channel_id=1, source_target_pairs={{0,4},{1,5},{2,6},{3,7},{4,0},{5,1},{6,2},{7,3},{8,12},{9,13},{10,... | collective-permute-start | bytes 393224 | tf_op jit(solution)/shard_map/ppermute | solution.py:658
  17.7 4.5 %collective-permute-start.10 = (f32[2,512]{1,0:T(2,128)S(1)}, f32[2,512]{1,0:T(2,128)S(1)}, u32[]{:S(2)}, u32[]{:S(2)}) collective-permute-start(f32[2,512]{1,0:T(2,128)S(1)} %pad_maximum_fusion.l0), channel_id=1, source_target_pairs={{0,3},{1,2},{2,1},{3,0},{4,7},{5,6},{6,5},{7,4},{8,11},{9,10},{10,... | collective-permute-start | bytes 12296 | tf_op jit(solution)/shard_map/ppermute | solution.py:658
  17.8 6.8 %collective-permute-start.8 = (f32[2,512]{1,0:T(2,128)S(1)}, f32[2,512]{1,0:T(2,128)S(1)}, u32[]{:S(2)}, u32[]{:S(2)}) collective-permute-start(f32[2,512]{1,0:T(2,128)S(1)} %pad_maximum_fusion.l0), channel_id=1, source_target_pairs={{0,1},{1,0},{2,3},{3,2},{4,5},{5,4},{6,7},{7,6},{8,9},{9,8},{10,11... | collective-permute-start | bytes 12296 | tf_op jit(solution)/shard_map/ppermute | solution.py:658
  19.4 7.1 %collective-permute-start.9 = (f32[2,512]{1,0:T(2,128)S(1)}, f32[2,512]{1,0:T(2,128)S(1)}, u32[]{:S(2)}, u32[]{:S(2)}) collective-permute-start(f32[2,512]{1,0:T(2,128)S(1)} %pad_maximum_fusion.l0), channel_id=1, source_target_pairs={{0,2},{1,3},{2,0},{3,1},{4,6},{5,7},{6,4},{7,5},{8,10},{9,11},{10,... | collective-permute-start | bytes 12296 | tf_op jit(solution)/shard_map/ppermute | solution.py:658
  21.7 11.9 %collective-permute-start.3 = (bf16[136,256]{1,0:T(8,128)(2,1)S(1)}, bf16[136,256]{1,0:T(8,128)(2,1)S(1)}, u32[]{:S(2)}, u32[]{:S(2)}) collective-permute-start(bf16[136,256]{1,0:T(8,128)(2,1)S(1)} %get-tuple-element.59), channel_id=1, source_target_pairs={{0,4},{1,5},{2,6},{3,7},{4,0},{5,1},{6,2},{7,3},{8,12},{9,13},{10,... | collective-permute-start | bytes 208904 | tf_op jit(solution)/shard_map/ppermute | solution.py:658
  22.3 11.3 %collective-permute-start.4 = (bf16[136,256]{1,0:T(8,128)(2,1)S(1)}, bf16[136,256]{1,0:T(8,128)(2,1)S(1)}, u32[]{:S(2)}, u32[]{:S(2)}) collective-permute-start(bf16[136,256]{1,0:T(8,128)(2,1)S(1)} %get-tuple-element.60), channel_id=1, source_target_pairs={{0,12},{1,13},{2,14},{3,15},{4,8},{5,9},{6,10},{7,11},{8,20},{9,21... | collective-permute-start | bytes 208904 | tf_op jit(solution)/shard_map/ppermute | solution.py:658
  24.6 9.0 %collective-permute-start.5 = (bf16[136,256]{1,0:T(8,128)(2,1)S(1)}, bf16[136,256]{1,0:T(8,128)(2,1)S(1)}, u32[]{:S(2)}, u32[]{:S(2)}) collective-permute-start(bf16[136,256]{1,0:T(8,128)(2,1)S(1)} %get-tuple-element.61), channel_id=1, source_target_pairs={{0,20},{1,21},{2,22},{3,23},{4,16},{5,17},{6,18},{7,19},{8,28},{9,... | collective-permute-start | bytes 208904 | tf_op jit(solution)/shard_map/ppermute | solution.py:658
  26.6 7.0 %collective-permute-start.6 = (bf16[136,256]{1,0:T(8,128)(2,1)S(1)}, bf16[136,256]{1,0:T(8,128)(2,1)S(1)}, u32[]{:S(2)}, u32[]{:S(2)}) collective-permute-start(bf16[136,256]{1,0:T(8,128)(2,1)S(1)} %get-tuple-element.62), channel_id=1, source_target_pairs={{0,28},{1,29},{2,30},{3,31},{4,24},{5,25},{6,26},{7,27},{8,4},{9,5... | collective-permute-start | bytes 208904 | tf_op jit(solution)/shard_map/ppermute | solution.py:658
  35.9 5.0 %collective-permute-start.11 = (bf16[512,128]{1,0:T(8,128)(2,1)S(1)}, bf16[512,128]{1,0:T(8,128)(2,1)S(1)}, u32[]{:S(2)}, u32[]{:S(2)}) collective-permute-start(bf16[512,128]{1,0:T(8,128)(2,1)S(1)} %get-tuple-element.70), channel_id=1, source_target_pairs={{0,4},{1,5},{2,6},{3,7},{4,0},{5,1},{6,2},{7,3},{8,12},{9,13},{10,... | collective-permute-start | bytes 393224 | tf_op jit(solution)/shard_map/ppermute | solution.py:658
  41.0 6.2 %collective-permute-start.12 = (bf16[128,256]{1,0:T(8,128)(2,1)S(1)}, bf16[128,256]{1,0:T(8,128)(2,1)S(1)}, u32[]{:S(2)}, u32[]{:S(2)}) collective-permute-start(bf16[128,256]{1,0:T(8,128)(2,1)S(1)} %get-tuple-element.72), channel_id=1, source_target_pairs={{0,8},{1,9},{2,10},{3,11},{4,12},{5,13},{6,14},{7,15},{8,16},{9,17... | collective-permute-start | bytes 196616 | tf_op jit(solution)/shard_map/ppermute | solution.py:658
  41.3 6.7 %collective-permute-start.13 = (bf16[128,256]{1,0:T(8,128)(2,1)S(1)}, bf16[128,256]{1,0:T(8,128)(2,1)S(1)}, u32[]{:S(2)}, u32[]{:S(2)}) collective-permute-start(bf16[128,256]{1,0:T(8,128)(2,1)S(1)} %get-tuple-element.73), channel_id=1, source_target_pairs={{0,16},{1,17},{2,18},{3,19},{4,20},{5,21},{6,22},{7,23},{8,24},{9,... | collective-permute-start | bytes 196616 | tf_op jit(solution)/shard_map/ppermute | solution.py:658
  44.4 4.3 %collective-permute-start.14 = (bf16[128,256]{1,0:T(8,128)(2,1)S(1)}, bf16[128,256]{1,0:T(8,128)(2,1)S(1)}, u32[]{:S(2)}, u32[]{:S(2)}) collective-permute-start(bf16[128,256]{1,0:T(8,128)(2,1)S(1)} %get-tuple-element.74), channel_id=1, source_target_pairs={{0,24},{1,25},{2,26},{3,27},{4,28},{5,29},{6,30},{7,31},{8,0},{9,1... | collective-permute-start | bytes 196616 | tf_op jit(solution)/shard_map/ppermute | solution.py:658
  57.9 7.1 %collective-permute-start.19 = (bf16[48,2048]{1,0:T(8,128)(2,1)S(1)}, bf16[48,2048]{1,0:T(8,128)(2,1)S(1)}, u32[]{:S(2)}, u32[]{:S(2)}) collective-permute-start(bf16[48,2048]{1,0:T(8,128)(2,1)S(1)} %get-tuple-element.81), channel_id=1, source_target_pairs={{0,2},{1,3},{2,0},{3,1},{4,6},{5,7},{6,4},{7,5},{8,10},{9,11},{10,... | collective-permute-start | bytes 589832 | tf_op jit(solution)/shard_map/ppermute | solution.py:658
  66.3 10.4 %collective-permute-start.21 = (bf16[48,2176]{1,0:T(8,128)(2,1)S(1)}, bf16[48,2176]{1,0:T(8,128)(2,1)S(1)}, u32[]{:S(2)}, u32[]{:S(2)}) collective-permute-start(bf16[48,2176]{1,0:T(8,128)(2,1)S(1)} %collective-permute-done.20.refs_0_.s0), channel_id=1, source_target_pairs={{0,4},{1,5},{2,6},{3,7},{4,0},{5,1},{6,2},{7,3},{8,12},{9,13},{10,... | collective-permute-start | bytes 626696 | tf_op jit(solution)/shard_map/ppermute | solution.py:658
  67.0 14.2 %collective-permute-start.22 = (bf16[48,2176]{1,0:T(8,128)(2,1)S(1)}, bf16[48,2176]{1,0:T(8,128)(2,1)S(1)}, u32[]{:S(2)}, u32[]{:S(2)}) collective-permute-start(bf16[48,2176]{1,0:T(8,128)(2,1)S(1)} %collective-permute-done.20.refs_0_.s0), channel_id=1, source_target_pairs={{0,2},{1,3},{2,0},{3,1},{4,6},{5,7},{6,4},{7,5},{8,10},{9,11},{10,... | collective-permute-start | bytes 626696 | tf_op jit(solution)/shard_map/ppermute | solution.py:658
  76.7 9.2 %collective-permute-start.23 = (bf16[48,2176]{1,0:T(8,128)(2,1)S(1)}, bf16[48,2176]{1,0:T(8,128)(2,1)S(1)}, u32[]{:S(2)}, u32[]{:S(2)}) collective-permute-start(bf16[48,2176]{1,0:T(8,128)(2,1)S(1)} %collective-permute-done.20.refs_0_.s0), channel_id=1, source_target_pairs={{0,1},{1,0},{2,3},{3,2},{4,5},{5,4},{6,7},{7,6},{8,9},{9,8},{10,11... | collective-permute-start | bytes 626696 | tf_op jit(solution)/shard_map/ppermute | solution.py:658
  76.7 9.2 %collective-permute-start.24 = (bf16[48,2176]{1,0:T(8,128)(2,1)S(1)}, bf16[48,2176]{1,0:T(8,128)(2,1)S(1)}, u32[]{:S(2)}, u32[]{:S(2)}) collective-permute-start(bf16[48,2176]{1,0:T(8,128)(2,1)S(1)} %collective-permute-done.21.refs_1_), channel_id=1, source_target_pairs={{0,1},{1,0},{2,3},{3,2},{4,5},{5,4},{6,7},{7,6},{8,9},{9,8},{10,11... | collective-permute-start | bytes 626696 | tf_op jit(solution)/shard_map/ppermute | solution.py:658
  81.2 4.7 %collective-permute-start.25 = (bf16[48,2176]{1,0:T(8,128)(2,1)S(1)}, bf16[48,2176]{1,0:T(8,128)(2,1)S(1)}, u32[]{:S(2)}, u32[]{:S(2)}) collective-permute-start(bf16[48,2176]{1,0:T(8,128)(2,1)S(1)} %collective-permute-done.22.refs_2_.s1), channel_id=1, source_target_pairs={{0,1},{1,0},{2,3},{3,2},{4,5},{5,4},{6,7},{7,6},{8,9},{9,8},{10,11... | collective-permute-start | bytes 626696 | tf_op jit(solution)/shard_map/ppermute | solution.py:658
  90.0 11.7 %collective-permute-start.26 = (bf16[288,1024]{1,0:T(8,128)(2,1)S(1)}, bf16[288,1024]{1,0:T(8,128)(2,1)S(1)}, u32[]{:S(2)}, u32[]{:S(2)}) collective-permute-start(bf16[288,1024]{1,0:T(8,128)(2,1)S(1)} %get-tuple-element.87), channel_id=1, source_target_pairs={{0,1},{1,0},{2,3},{3,2},{4,5},{5,4},{6,7},{7,6},{8,9},{9,8},{10,11... | collective-permute-start | bytes 1769480 | tf_op jit(solution)/shard_map/ppermute | solution.py:658
  90.5 7.3 %collective-permute-start.29 = (bf16[48,2176]{1,0:T(8,128)(2,1)S(1)}, bf16[48,2176]{1,0:T(8,128)(2,1)S(1)}, u32[]{:S(2)}, u32[]{:S(2)}) collective-permute-start(bf16[48,2176]{1,0:T(8,128)(2,1)S(1)} %collective-permute-done.21.refs_1_), channel_id=1, source_target_pairs={{0,2},{1,3},{2,0},{3,1},{4,6},{5,7},{6,4},{7,5},{8,10},{9,11},{10,... | collective-permute-start | bytes 626696 | tf_op jit(solution)/shard_map/ppermute | solution.py:658
  101.8 13.6 %collective-permute-start.27 = (bf16[192,512]{1,0:T(8,128)(2,1)S(1)}, bf16[192,512]{1,0:T(8,128)(2,1)S(1)}, u32[]{:S(2)}, u32[]{:S(2)}) collective-permute-start(bf16[192,512]{1,0:T(8,128)(2,1)S(1)} %get-tuple-element.89), channel_id=1, source_target_pairs={{0,2},{1,3},{2,0},{3,1},{4,6},{5,7},{6,4},{7,5},{8,10},{9,11},{10,... | collective-permute-start | bytes 589832 | tf_op jit(solution)/shard_map/ppermute | solution.py:658
  103.7 5.3 %collective-permute-start.32 = (bf16[96,512]{1,0:T(8,128)(2,1)S(1)}, bf16[96,512]{1,0:T(8,128)(2,1)S(1)}, u32[]{:S(2)}, u32[]{:S(2)}) collective-permute-start(bf16[96,512]{1,0:T(8,128)(2,1)S(1)} %get-tuple-element.94), channel_id=1, source_target_pairs={{0,4},{1,5},{2,6},{3,7},{4,0},{5,1},{6,2},{7,3},{8,12},{9,13},{10,... | collective-permute-start | bytes 294920 | tf_op jit(solution)/shard_map/ppermute | solution.py:658
  105.1 6.9 %collective-permute-start.33 = (bf16[96,512]{1,0:T(8,128)(2,1)S(1)}, bf16[96,512]{1,0:T(8,128)(2,1)S(1)}, u32[]{:S(2)}, u32[]{:S(2)}) collective-permute-start(bf16[96,512]{1,0:T(8,128)(2,1)S(1)} %get-tuple-element.95), channel_id=1, source_target_pairs={{0,6},{1,7},{2,4},{3,5},{4,2},{5,3},{6,0},{7,1},{8,14},{9,15},{10,... | collective-permute-start | bytes 294920 | tf_op jit(solution)/shard_map/ppermute | solution.py:658
  106.3 7.1 %collective-permute-start.28 = (bf16[96,512]{1,0:T(8,128)(2,1)S(1)}, bf16[96,512]{1,0:T(8,128)(2,1)S(1)}, u32[]{:S(2)}, u32[]{:S(2)}) collective-permute-start(bf16[96,512]{1,0:T(8,128)(2,1)S(1)} %get-tuple-element.90), channel_id=1, source_target_pairs={{0,4},{1,5},{2,6},{3,7},{4,0},{5,1},{6,2},{7,3},{8,12},{9,13},{10,... | collective-permute-start | bytes 294920 | tf_op jit(solution)/shard_map/ppermute | solution.py:658
  107.6 7.8 %collective-permute-start.34 = (bf16[96,512]{1,0:T(8,128)(2,1)S(1)}, bf16[96,512]{1,0:T(8,128)(2,1)S(1)}, u32[]{:S(2)}, u32[]{:S(2)}) collective-permute-start(bf16[96,512]{1,0:T(8,128)(2,1)S(1)} %get-tuple-element.96), channel_id=1, source_target_pairs={{0,6},{1,7},{2,4},{3,5},{4,2},{5,3},{6,0},{7,1},{8,14},{9,15},{10,... | collective-permute-start | bytes 294920 | tf_op jit(solution)/shard_map/ppermute | solution.py:658
  116.3 3.7 %collective-permute-start.36 = (f32[8,256]{1,0:T(8,128)S(1)}, f32[8,256]{1,0:T(8,128)S(1)}, u32[]{:S(2)}, u32[]{:S(2)}) collective-permute-start(f32[8,256]{1,0:T(8,128)S(1)} %get-tuple-element.98.refs_1_), channel_id=1, source_target_pairs={{0,2},{1,3},{2,0},{3,1},{4,6},{5,7},{6,4},{7,5},{8,10},{9,11},{10,... | collective-permute-start | bytes 24584 | tf_op jit(solution)/shard_map/ppermute | solution.py:658
  120.5 6.5 %collective-permute-start.38 = (bf16[48,512]{1,0:T(8,128)(2,1)S(1)}, bf16[48,512]{1,0:T(8,128)(2,1)S(1)}, u32[]{:S(2)}, u32[]{:S(2)}) collective-permute-start(bf16[48,512]{1,0:T(8,128)(2,1)S(1)} %get-tuple-element.100), channel_id=1, source_target_pairs={{0,8},{1,9},{2,10},{3,11},{4,12},{5,13},{6,14},{7,15},{8,16},{9,17... | collective-permute-start | bytes 147464 | tf_op jit(solution)/shard_map/ppermute | solution.py:658
  120.8 7.5 %collective-permute-start.39 = (bf16[48,512]{1,0:T(8,128)(2,1)S(1)}, bf16[48,512]{1,0:T(8,128)(2,1)S(1)}, u32[]{:S(2)}, u32[]{:S(2)}) collective-permute-start(bf16[48,512]{1,0:T(8,128)(2,1)S(1)} %get-tuple-element.101), channel_id=1, source_target_pairs={{0,16},{1,17},{2,18},{3,19},{4,20},{5,21},{6,22},{7,23},{8,24},{9,... | collective-permute-start | bytes 147464 | tf_op jit(solution)/shard_map/ppermute | solution.py:658
  123.2 5.0 %collective-permute-start.40 = (bf16[48,512]{1,0:T(8,128)(2,1)S(1)}, bf16[48,512]{1,0:T(8,128)(2,1)S(1)}, u32[]{:S(2)}, u32[]{:S(2)}) collective-permute-start(bf16[48,512]{1,0:T(8,128)(2,1)S(1)} %get-tuple-element.102), channel_id=1, source_target_pairs={{0,24},{1,25},{2,26},{3,27},{4,28},{5,29},{6,30},{7,31},{8,0},{9,1... | collective-permute-start | bytes 147464 | tf_op jit(solution)/shard_map/ppermute | solution.py:658
  (13 other events, 103.2 us)

commit v2 on v1

--- a/solution.py
+++ b/solution.py
@@ -407,13 +407,13 @@
         out[d * rows : (d + 1) * rows, :] = value.astype(BF)
 
 
-def attend_one_kernel(planes, spare, *refs):
+def attend_one_kernel(planes, *refs):
     same, cross = refs[:planes], refs[planes : 2 * planes]
     refs = refs[2 * planes :]
-    out, *held = refs[1 + spare : 6 + spare]
+    out, *held = refs[1:6]
     gather_kernel(planes, same, cross, refs[0], *held)
     side = 1 - lax.axis_index("sp") % 2
-    attend_half(planes, side, *held, out, *refs[6 + spare :])
+    attend_half(planes, side, *held, out, *refs[6:])
 
 
 def attend_two_kernel(planes, *refs):
@@ -440,18 +440,10 @@
         for k in range(2):
             at = pl.ds(pl.multiple_of(k * width + u * lane, lane), lane)
             out[:, at] = parts[d][:, k * lane : (k + 1) * lane]
-    ones = jnp.ones((8, width), F32)
     whole = out[...].astype(F32)
     for k in range(2):
         part = whole[:, k * width : (k + 1) * width]
-        line = lax.dot_general(
-            ones,
-            part * part,
-            (((1,), (1,)), ((), ())),
-            precision=lax.Precision.HIGHEST,
-            preferred_element_type=F32,
-        )
-        sums[k : k + 1, :] = line[0:1]
+        sums[k : k + 1, :] = row_sums(part * part)
     sums[2:8, :] = jnp.zeros((6, sums.shape[1]), F32)
     out[...] = (whole * gains[0:1, :]).astype(BF)
 
@@ -494,6 +486,13 @@
     out[:, columns : columns + LANE] = w[...]
 
 
+def row_sums(v):
+    n = v.shape[0]
+    column = jnp.sum(v, axis=1, keepdims=True)
+    eye = iota((n, n), 0) == iota((n, n), 1)
+    return jnp.sum(jnp.where(eye, column, 0.0), axis=0, keepdims=True)
+
+
 def row_norm(total, gain, bias):
     columns = total.shape[1]
     mean = jnp.sum(total, axis=1, keepdims=True) / columns
@@ -575,16 +574,8 @@
         start = pl.multiple_of((2 * dc + dy) * n, 16)
         second[k * n : (k + 1) * n, :] = routed_s[pl.ds(start, n), :]
     value = second[...]
-    ones = jnp.ones((8, width), F32)
     for k, part in enumerate((value, value * value)):
-        line = lax.dot_general(
-            ones,
-            part,
-            (((1,), (1,)), ((), ())),
-            precision=lax.Precision.HIGHEST,
-            preferred_element_type=F32,
-        )
-        sums[k : k + 1, 0 : 4 * n] = line[0:1]
+        sums[k : k + 1, 0 : 4 * n] = row_sums(part)
 
 
 def finish_kernel(columns, second, c0, c1, c2, c3, lines, f0, f1, f2, f3, all_s):
@@ -694,13 +685,6 @@
     (values,) = call(relay_kernel, [shape_of((planes * rows, LANE))], got_same, 4)
     relayed = swap_plane(values, 1, 0)
 
-    m, n, w = call(
-        lambda *refs: route_kernel(cap, *refs),
-        [shape_of((4 * cap, rows)), shape_of((rows, 4 * cap)), shape_of((cap, LANE))],
-        (*in_hbm(jnp.transpose(expert_ids), jnp.transpose(route_weight)), got_same[2]),
-        8,
-        hidden=1,
-    )
     own_lines = jnp.stack([gain_settle, bias_settle])
     lines = [own_lines] + [swap_tp(own_lines, k) for k in range(1, 4)]
 
@@ -716,21 +700,17 @@
             compiler_params=pltpu.CompilerParams(vmem_limit_bytes=16 << 20),
         )(*in_hbm(*weights), after)
 
-    p_alpha, p_beta = load((project_alpha, project_beta), got_same[2])
-
     total = chips * rows
-    spare = (m, n, w, *lines[1:], p_alpha)
     work = [
         pltpu.VMEM((2, planes * rows, LANE), F32),
         pltpu.VMEM((2 * rows, 2 * rows), BF),
     ]
     half = shape_of((planes * rows, LANE))
     other_x, *held = call(
-        lambda *refs: attend_one_kernel(planes, len(spare), *refs),
+        lambda *refs: attend_one_kernel(planes, *refs),
         [half, shape_of((2, total, LANE)), shape_of((total, LANE)), shape_of((total, LANE)), shape_of((8, total), F32)],
-        (*got_same, *got_cross, relayed, *spare),
+        (*got_same, *got_cross, relayed),
         12,
-        hidden=len(spare),
         scratch=work,
     )
     got_x = swap_plane(other_x, 1, 0)
@@ -738,7 +718,22 @@
         lambda *refs: attend_two_kernel(planes, *refs), [half], tuple(held), 12, scratch=work
     )
     merged = call(merge_kernel, [shape_of((rows, 2 * LANE))] * planes, (own_x, got_x), 4)
-    back = [merged[0]] + [shift(merged[d], d, 0) for d in range(1, planes)]
+
+    def to_planes(pieces):
+        got = [pieces[0]]
+        for d in range(1, planes):
+            got.append(shift(pieces[d], d, 0))
+        return got
+
+    back = to_planes(merged)
+    p_alpha, p_beta = load((project_alpha, project_beta), own_x)
+    m, n, w = call(
+        lambda *refs: route_kernel(cap, *refs),
+        [shape_of((4 * cap, rows)), shape_of((rows, 4 * cap)), shape_of((cap, LANE))],
+        (*in_hbm(jnp.transpose(expert_ids), jnp.transpose(route_weight)), own_x),
+        8,
+        hidden=1,
+    )
     gains = jnp.concatenate([gain_alpha, gain_beta])[None, :]
     att, sums = call(
         lambda *refs: collect_kernel(planes, *refs),
@@ -762,8 +757,8 @@
         8,
     )
     got = swap_tp(send, 2)
-    e_gate, e_up, e_down = load((expert_gate, expert_up, expert_down), keep)
-    settled, _ = call(
+    e_gate, e_up = load((expert_gate, expert_up), keep)
+    settled, all_lines = call(
         settle_kernel,
         [shape_of((cap, columns + LANE)), shape_of((2, columns), F32)],
         (own, got, w, *lines),
@@ -775,6 +770,7 @@
         return g, x, 2 * (t >> 1) + (z >> 1)
 
     mine = move(settled, to_plane)
+    (e_down,) = load((expert_down,), all_lines)
     from_x, from_y = swap_plane(mine, 1, 0), swap_plane(mine, 0, 2)
     from_xy = swap_plane(from_x, 0, 2)
     near = [mine, from_x, from_y]
@@ -831,7 +827,7 @@
         8,
         scratch=[pltpu.VMEM((4 * cap, width), BF)],
     )
-    home = [ends[0]] + [shift(ends[d], d, 0) for d in range(1, planes)]
+    home = to_planes(ends)
     (out,) = call(place_kernel, [shape_of((rows, width))], (n, *home), 4)
     return out
 

time: 129 us -> 129 us (level)
  waiting for transfers between devices: 44.6 us -> 47 us
  starting transfers between devices: 55.4 us -> 53.6 us
    ppermute x41, waiting for transfers between devices: 44.6 us -> 47 us  [move(): return lax.ppermute(v, ('sp', 'tp'), perm)]
    ppermute x41, starting transfers between devices: 55.4 us -> 53.6 us  [move(): return lax.ppermute(v, ('sp', 'tp'), perm)]
    pallas_call x18, Pallas kernels: 21.1 us -> 19.6 us  [call(): pl.pallas_call(kernel, out_shape=outs, in_specs=[local] * (len(args) - hi...]
    pallas_call x2 -> x3, Pallas kernels: 6.95 us -> 7.92 us  [load(): pl.pallas_call(lambda *refs: load_kernel(*refs[:count], *refs[count + 1:]...]
  transfers between devices with their start and end apart: 41 -> 41, of which waited for: 21 -> 21; matrix products, arithmetic and copies ran while one was open for 1% -> 0% of each run, Pallas kernels for 11% -> 12%
where the time goes in v2:
time: 129 us
  starting transfers between devices  53.6 us (42%)
  waiting for transfers between devices  47 us (36%)
  Pallas kernels  27.6 us (21%)
    ppermute x41, starting transfers between devices, move(): return lax.ppermute(v, ('sp', 'tp'), perm)  53.6 us
    ppermute x41, waiting for transfers between devices, move(): return lax.ppermute(v, ('sp', 'tp'), perm)  47 us
    pallas_call x18, Pallas kernels, call(): pl.pallas_call(kernel, out_shape=outs, in_specs=[local] * (len(args) - hi...  19.6 us
    pallas_call x3, Pallas kernels, load(): pl.pallas_call(lambda *refs: load_kernel(*refs[:count], *refs[count + 1:]...  7.92 us
  transfers between devices with their start and end apart: 41, of which 21 were waited for; matrix products, arithmetic and copies ran while one was open for 0% of the time, Pallas kernels for 12%

profile of v2, /device:TPU:0, one launch (start us, length us, event | category | flops | bytes accessed | tf_op | source)
XLA Modules:
  0.0 128.5 jit_solution(8519221705038168156)
XLA Ops:
  0.0 2.3 %shard_map.190 = (bf16[136,384]{1,0:T(8,128)(2,1)S(1)}, bf16[136,384]{1,0:T(8,128)(2,1)S(1)}, bf16[136,384]{1,0:T(8,128)(2,1)S(1)}, bf16[136,384]{1,0:T(8,128)(2,1)S(1)}) custom-call(bf16[128,512]{1,0:T(8,128)(2,1)} %refs_0_.6, bf16[128,4,128]{2,1,0:T(4,128)(2,1)} %refs_1_.5, bf16[128,512]{1,0:T(8,128)(2,1)} %refs_2_.4, bf16[128,4,256]{2,1,0:T(4,128)(2,1)} %refs_3_.3, ...), custom_call_target="tpu_custom_call" | custom-call | tf_op jit(solution)/shard_map/pallas_call | solution.py:203
  2.3 3.1 %collective-permute-start = (bf16[136,384]{1,0:T(8,128)(2,1)S(1)}, bf16[136,384]{1,0:T(8,128)(2,1)S(1)}, u32[]{:S(2)}, u32[]{:S(2)}) collective-permute-start(bf16[136,384]{1,0:T(8,128)(2,1)S(1)} %get-tuple-element.55), channel_id=1, source_target_pairs={{0,8},{1,9},{2,10},{3,11},{4,12},{5,13},{6,14},{7,15},{8,16},{9,17... | collective-permute-start | bytes 313352 | tf_op jit(solution)/shard_map/ppermute | solution.py:649
  5.4 2.6 %collective-permute-start.1 = (bf16[136,384]{1,0:T(8,128)(2,1)S(1)}, bf16[136,384]{1,0:T(8,128)(2,1)S(1)}, u32[]{:S(2)}, u32[]{:S(2)}) collective-permute-start(bf16[136,384]{1,0:T(8,128)(2,1)S(1)} %get-tuple-element.56), channel_id=1, source_target_pairs={{0,16},{1,17},{2,18},{3,19},{4,20},{5,21},{6,22},{7,23},{8,24},{9,... | collective-permute-start | bytes 313352 | tf_op jit(solution)/shard_map/ppermute | solution.py:649
  9.3 2.0 %collective-permute-done.refs_1_ = bf16[136,384]{1,0:T(8,128)(2,1)S(1)} collective-permute-done((bf16[136,384]{1,0:T(8,128)(2,1)S(1)}, bf16[136,384]{1,0:T(8,128)(2,1)S(1)}, u32[]{:S(2)}, u32[]{:S(2)}) %collective-permute-start) | collective-permute-done | bytes 104480 | tf_op jit(solution)/shard_map/ppermute | solution.py:649
  11.3 3.7 %collective-permute-done.1.refs_2_ = bf16[136,384]{1,0:T(8,128)(2,1)S(1)} collective-permute-done((bf16[136,384]{1,0:T(8,128)(2,1)S(1)}, bf16[136,384]{1,0:T(8,128)(2,1)S(1)}, u32[]{:S(2)}, u32[]{:S(2)}) %collective-permute-start.1) | collective-permute-done | bytes 104480 | tf_op jit(solution)/shard_map/ppermute | solution.py:649
  16.6 1.8 %shard_map.191 = (bf16[136,256]{1,0:T(8,128)(2,1)S(1)}, bf16[136,256]{1,0:T(8,128)(2,1)S(1)}, bf16[136,256]{1,0:T(8,128)(2,1)S(1)}, bf16[136,256]{1,0:T(8,128)(2,1)S(1)}) custom-call(bf16[128,512]{1,0:T(8,128)(2,1)} %refs_0_.6, bf16[128,4,128]{2,1,0:T(4,128)(2,1)} %refs_1_.5, bf16[128,512]{1,0:T(8,128)(2,1)} %refs_2_.4, bf16[128,4,256]{2,1,0:T(4,128)(2,1)} %refs_3_.3, ...), custom_call_target="tpu_custom_call" | custom-call | tf_op jit(solution)/shard_map/pallas_call | solution.py:203
  18.9 3.6 %collective-permute-start.4 = (bf16[136,256]{1,0:T(8,128)(2,1)S(1)}, bf16[136,256]{1,0:T(8,128)(2,1)S(1)}, u32[]{:S(2)}, u32[]{:S(2)}) collective-permute-start(bf16[136,256]{1,0:T(8,128)(2,1)S(1)} %get-tuple-element.59), channel_id=1, source_target_pairs={{0,12},{1,13},{2,14},{3,15},{4,8},{5,9},{6,10},{7,11},{8,20},{9,21... | collective-permute-start | bytes 208904 | tf_op jit(solution)/shard_map/ppermute | solution.py:649
  26.7 2.8 %collective-permute-done.5.refs_6_ = bf16[136,256]{1,0:T(8,128)(2,1)S(1)} collective-permute-done((bf16[136,256]{1,0:T(8,128)(2,1)S(1)}, bf16[136,256]{1,0:T(8,128)(2,1)S(1)}, u32[]{:S(2)}, u32[]{:S(2)}) %collective-permute-start.5) | collective-permute-done | bytes 69664 | tf_op jit(solution)/shard_map/ppermute | solution.py:649
  29.8 2.2 %shard_map.193 = (bf16[512,128]{1,0:T(8,128)(2,1)S(1)}, bf16[2,1024,128]{2,1,0:T(8,128)(2,1)S(1)}, bf16[1024,128]{1,0:T(8,128)(2,1)S(1)}, bf16[1024,128]{1,0:T(8,128)(2,1)S(1)}, f32[8,1024]{1,0:T(8,128)S(1)}) custom-call(bf16[136,384]{1,0:T(8,128)(2,1)S(1)} %get-tuple-element.54.refs_0_, bf16[136,384]{1,0:T(8,128)(2,1)S(1)} %collective-permute-done.refs_1_, ...), custom_call_target="tpu_custom_call" | custom-call | tf_op jit(solution)/shard_map/pallas_call | solution.py:203
  32.4 2.1 %shard_map.194.refs_2_.own = bf16[512,128]{1,0:T(8,128)(2,1)S(1)} custom-call(bf16[2,1024,128]{2,1,0:T(8,128)(2,1)S(1)} %get-tuple-element.62.refs_0_, bf16[1024,128]{1,0:T(8,128)(2,1)S(1)} %get-tuple-element.63.refs_1_, bf16[1024,128]{1,0:T(8,128)(2,1)S(1)} %get-tuple-element.64.refs_2_, f32[8,1024]{1,0:T(8,128)S(1)} %get-tuple-element.65.refs_3_), custom_call_target="tpu_custom_call" | custom-call | tf_op jit(solution)/shard_map/pallas_call | solution.py:203
  34.5 2.5 %collective-permute-done.8.got = bf16[512,128]{1,0:T(8,128)(2,1)S(1)} collective-permute-done((bf16[512,128]{1,0:T(8,128)(2,1)S(1)}, bf16[512,128]{1,0:T(8,128)(2,1)S(1)}, u32[]{:S(2)}, u32[]{:S(2)}) %collective-permute-start.8) | collective-permute-done | bytes 131104 | tf_op jit(solution)/shard_map/ppermute | solution.py:649
  38.4 2.2 %collective-permute-start.11 = (bf16[128,256]{1,0:T(8,128)(2,1)S(1)}, bf16[128,256]{1,0:T(8,128)(2,1)S(1)}, u32[]{:S(2)}, u32[]{:S(2)}) collective-permute-start(bf16[128,256]{1,0:T(8,128)(2,1)S(1)} %get-tuple-element.71), channel_id=1, source_target_pairs={{0,24},{1,25},{2,26},{3,27},{4,28},{5,29},{6,30},{7,31},{8,0},{9,1... | collective-permute-start | bytes 196616 | tf_op jit(solution)/shard_map/ppermute | solution.py:649
  40.6 2.7 %collective-permute-done.10.refs_2_ = bf16[128,256]{1,0:T(8,128)(2,1)S(1)} collective-permute-done((bf16[128,256]{1,0:T(8,128)(2,1)S(1)}, bf16[128,256]{1,0:T(8,128)(2,1)S(1)}, u32[]{:S(2)}, u32[]{:S(2)}) %collective-permute-start.10) | collective-permute-done | bytes 65568 | tf_op jit(solution)/shard_map/ppermute | solution.py:649
  43.4 3.3 %collective-permute-done.9.refs_1_ = bf16[128,256]{1,0:T(8,128)(2,1)S(1)} collective-permute-done((bf16[128,256]{1,0:T(8,128)(2,1)S(1)}, bf16[128,256]{1,0:T(8,128)(2,1)S(1)}, u32[]{:S(2)}, u32[]{:S(2)}) %collective-permute-start.9) | collective-permute-done | bytes 65568 | tf_op jit(solution)/shard_map/ppermute | solution.py:649
  47.0 1.6 %collective-permute-start.13 = (f32[8,128]{1,0:T(8,128)S(1)}, f32[8,128]{1,0:T(8,128)S(1)}, u32[]{:S(2)}, u32[]{:S(2)}) collective-permute-start(f32[8,128]{1,0:T(8,128)S(1)} %get-tuple-element.74.refs_3_), channel_id=1, source_target_pairs={{0,2},{1,3},{2,0},{3,1},{4,6},{5,7},{6,4},{7,5},{8,10},{9,11},{10,... | collective-permute-start | bytes 12296 | tf_op jit(solution)/shard_map/ppermute | solution.py:649
  48.9 2.2 %shard_map.198 = (bf16[512,2048]{1,0:T(8,128)(2,1)S(1)}, bf16[512,2048]{1,0:T(8,128)(2,1)S(1)}) custom-call(bf16[512,2048]{1,0:T(8,128)(2,1)} %refs_0_.7, bf16[512,2048]{1,0:T(8,128)(2,1)} %refs_1_.6, bf16[512,128]{1,0:T(8,128)(2,1)S(1)} %shard_map.194.refs_2_.own), custom_call_target="tpu_custom_call" | custom-call | tf_op jit(solution)/shard_map/pallas_call | solution.py:694
  52.1 2.1 %shard_map.199 = (bf16[96,2048]{1,0:T(8,128)(2,1)S(1)}, bf16[96,2048]{1,0:T(8,128)(2,1)S(1)}) custom-call(bf16[128,1024]{1,0:T(8,128)(2,1)S(1)} %get-tuple-element.72.refs_0_, bf16[192,128]{1,0:T(8,128)(2,1)S(1)} %get-tuple-element.73.refs_1_, bf16[128,512]{1,0:T(8,128)(2,1)} %refs_2_.5, f32[8,128]{1,0:T(8,128)S(1)} %get-tuple-element.74.refs_3_, ...), custom_call_target="tpu_custom_call" | custom-call | tf_op jit(solution)/shard_map/pallas_call | solution.py:203
  59.6 3.8 %collective-permute-done.18.l2 = f32[2,512]{1,0:T(2,128)S(1)} collective-permute-done((f32[2,512]{1,0:T(2,128)S(1)}, f32[2,512]{1,0:T(2,128)S(1)}, u32[]{:S(2)}, u32[]{:S(2)}) %collective-permute-start.18) | collective-permute-done | bytes 4128 | tf_op jit(solution)/shard_map/ppermute | solution.py:649
  65.4 10.7 %collective-permute-start.22 = (bf16[48,2176]{1,0:T(8,128)(2,1)S(1)}, bf16[48,2176]{1,0:T(8,128)(2,1)S(1)}, u32[]{:S(2)}, u32[]{:S(2)}) collective-permute-start(bf16[48,2176]{1,0:T(8,128)(2,1)S(1)} %collective-permute-done.20.refs_0_.s0), channel_id=1, source_target_pairs={{0,2},{1,3},{2,0},{3,1},{4,6},{5,7},{6,4},{7,5},{8,10},{9,11},{10,... | collective-permute-start | bytes 626696 | tf_op jit(solution)/shard_map/ppermute | solution.py:649
  76.6 3.7 %collective-permute-done.22.refs_2_.s1 = bf16[48,2176]{1,0:T(8,128)(2,1)S(1)} collective-permute-done((bf16[48,2176]{1,0:T(8,128)(2,1)S(1)}, bf16[48,2176]{1,0:T(8,128)(2,1)S(1)}, u32[]{:S(2)}, u32[]{:S(2)}) %collective-permute-start.22) | collective-permute-done | bytes 208928 | tf_op jit(solution)/shard_map/ppermute | solution.py:649
  80.3 3.5 %shard_map.202 = (bf16[1,2048,1024]{2,1,0:T(8,128)(2,1)S(1)}, bf16[1,2048,1024]{2,1,0:T(8,128)(2,1)S(1)}) custom-call(bf16[1,2048,1024]{2,1,0:T(8,128)(2,1)} %refs_0_.8, bf16[1,2048,1024]{2,1,0:T(8,128)(2,1)} %refs_1_.7, bf16[96,2048]{1,0:T(8,128)(2,1)S(1)} %get-tuple-element.77.keep.refs_2_), custom_call_target="tpu_custom_call" | custom-call | tf_op jit(solution)/shard_map/pallas_call | solution.py:694
  83.8 2.2 %shard_map.203.refs_8_.refs_4_ = bf16[1,1024,2048]{2,1,0:T(8,128)(2,1)S(1)} custom-call(bf16[1,1024,2048]{2,1,0:T(8,128)(2,1)} %refs_0_.9, f32[2,2048]{1,0:T(2,128)S(1)} %get-tuple-element.85.refs_1_), custom_call_target="tpu_custom_call" | custom-call | tf_op jit(solution)/shard_map/pallas_call | solution.py:694
  86.1 4.0 %shard_map.204 = (bf16[288,1024]{1,0:T(8,128)(2,1)S(1)}, bf16[288,1024]{1,0:T(8,128)(2,1)S(1)}) custom-call(bf16[48,2176]{1,0:T(8,128)(2,1)S(1)} %collective-permute-done.20.refs_0_.s0, bf16[48,2176]{1,0:T(8,128)(2,1)S(1)} %collective-permute-done.21.refs_1_, bf16[48,2176]{1,0:T(8,128)(2,1)S(1)} %collective-permute-done.22.refs_2_.s1, ...), custom_call_target="tpu_custom_call" | custom-call | tf_op jit(solution)/shard_map/pallas_call | solution.py:203
  90.7 1.7 %collective-permute-start.29 = (bf16[48,2176]{1,0:T(8,128)(2,1)S(1)}, bf16[48,2176]{1,0:T(8,128)(2,1)S(1)}, u32[]{:S(2)}, u32[]{:S(2)}) collective-permute-start(bf16[48,2176]{1,0:T(8,128)(2,1)S(1)} %collective-permute-done.21.refs_1_), channel_id=1, source_target_pairs={{0,2},{1,3},{2,0},{3,1},{4,6},{5,7},{6,4},{7,5},{8,10},{9,11},{10,... | collective-permute-start | bytes 626696 | tf_op jit(solution)/shard_map/ppermute | solution.py:649
  92.4 5.4 %collective-permute-done.29.refs_0_ = bf16[48,2176]{1,0:T(8,128)(2,1)S(1)} collective-permute-done((bf16[48,2176]{1,0:T(8,128)(2,1)S(1)}, bf16[48,2176]{1,0:T(8,128)(2,1)S(1)}, u32[]{:S(2)}, u32[]{:S(2)}) %collective-permute-start.29) | collective-permute-done | bytes 208928 | tf_op jit(solution)/shard_map/ppermute | solution.py:649
  99.3 2.2 %shard_map.206 = (bf16[96,1024]{1,0:T(8,128)(2,1)S(1)}, bf16[96,1024]{1,0:T(8,128)(2,1)S(1)}) custom-call(bf16[48,2176]{1,0:T(8,128)(2,1)S(1)} %collective-permute-done.29.refs_0_, bf16[48,2176]{1,0:T(8,128)(2,1)S(1)} %collective-permute-done.30.refs_1_, bf16[1,2048,1024]{2,1,0:T(8,128)(2,1)S(1)} %get-tuple-element.83.refs_6_.refs_2_, ...), custom_call_target="tpu_custom_call" | custom-call | tf_op jit(solution)/shard_map/pallas_call | solution.py:203
  101.8 1.8 %collective-permute-start.27 = (bf16[192,512]{1,0:T(8,128)(2,1)S(1)}, bf16[192,512]{1,0:T(8,128)(2,1)S(1)}, u32[]{:S(2)}, u32[]{:S(2)}) collective-permute-start(bf16[192,512]{1,0:T(8,128)(2,1)S(1)} %get-tuple-element.89), channel_id=1, source_target_pairs={{0,2},{1,3},{2,0},{3,1},{4,6},{5,7},{6,4},{7,5},{8,10},{9,11},{10,... | collective-permute-start | bytes 589832 | tf_op jit(solution)/shard_map/ppermute | solution.py:649
  109.3 2.7 %collective-permute-done.33.gxy0 = bf16[96,512]{1,0:T(8,128)(2,1)S(1)} collective-permute-done((bf16[96,512]{1,0:T(8,128)(2,1)S(1)}, bf16[96,512]{1,0:T(8,128)(2,1)S(1)}, u32[]{:S(2)}, u32[]{:S(2)}) %collective-permute-start.33) | collective-permute-done | bytes 98336 | tf_op jit(solution)/shard_map/ppermute | solution.py:649
  113.5 1.9 %collective-permute-done.34.gxy1 = bf16[96,512]{1,0:T(8,128)(2,1)S(1)} collective-permute-done((bf16[96,512]{1,0:T(8,128)(2,1)S(1)}, bf16[96,512]{1,0:T(8,128)(2,1)S(1)}, u32[]{:S(2)}, u32[]{:S(2)}) %collective-permute-start.34) | collective-permute-done | bytes 98336 | tf_op jit(solution)/shard_map/ppermute | solution.py:649
  117.7 1.8 %collective-permute-done.36.refs_3_ = f32[8,256]{1,0:T(8,128)S(1)} collective-permute-done((f32[8,256]{1,0:T(8,128)S(1)}, f32[8,256]{1,0:T(8,128)S(1)}, u32[]{:S(2)}, u32[]{:S(2)}) %collective-permute-start.36) | collective-permute-done | bytes 8224 | tf_op jit(solution)/shard_map/ppermute | solution.py:649
  121.1 2.8 %collective-permute-start.40 = (bf16[48,512]{1,0:T(8,128)(2,1)S(1)}, bf16[48,512]{1,0:T(8,128)(2,1)S(1)}, u32[]{:S(2)}, u32[]{:S(2)}) collective-permute-start(bf16[48,512]{1,0:T(8,128)(2,1)S(1)} %get-tuple-element.102), channel_id=1, source_target_pairs={{0,24},{1,25},{2,26},{3,27},{4,28},{5,29},{6,30},{7,31},{8,0},{9,1... | collective-permute-start | bytes 147464 | tf_op jit(solution)/shard_map/ppermute | solution.py:649
  123.9 2.6 %collective-permute-done.38.f1 = bf16[48,512]{1,0:T(8,128)(2,1)S(1)} collective-permute-done((bf16[48,512]{1,0:T(8,128)(2,1)S(1)}, bf16[48,512]{1,0:T(8,128)(2,1)S(1)}, u32[]{:S(2)}, u32[]{:S(2)}) %collective-permute-start.38) | collective-permute-done | bytes 49184 | tf_op jit(solution)/shard_map/ppermute | solution.py:649
  (86 shorter events, 34.4 us)
Async XLA Ops:
  2.3 9.0 %collective-permute-start = (bf16[136,384]{1,0:T(8,128)(2,1)S(1)}, bf16[136,384]{1,0:T(8,128)(2,1)S(1)}, u32[]{:S(2)}, u32[]{:S(2)}) collective-permute-start(bf16[136,384]{1,0:T(8,128)(2,1)S(1)} %get-tuple-element.55), channel_id=1, source_target_pairs={{0,8},{1,9},{2,10},{3,11},{4,12},{5,13},{6,14},{7,15},{8,16},{9,17... | collective-permute-start | bytes 313352 | tf_op jit(solution)/shard_map/ppermute | solution.py:649
  5.4 9.6 %collective-permute-start.1 = (bf16[136,384]{1,0:T(8,128)(2,1)S(1)}, bf16[136,384]{1,0:T(8,128)(2,1)S(1)}, u32[]{:S(2)}, u32[]{:S(2)}) collective-permute-start(bf16[136,384]{1,0:T(8,128)(2,1)S(1)} %get-tuple-element.56), channel_id=1, source_target_pairs={{0,16},{1,17},{2,18},{3,19},{4,20},{5,21},{6,22},{7,23},{8,24},{9,... | collective-permute-start | bytes 313352 | tf_op jit(solution)/shard_map/ppermute | solution.py:649
  8.0 7.0 %collective-permute-start.2 = (bf16[136,384]{1,0:T(8,128)(2,1)S(1)}, bf16[136,384]{1,0:T(8,128)(2,1)S(1)}, u32[]{:S(2)}, u32[]{:S(2)}) collective-permute-start(bf16[136,384]{1,0:T(8,128)(2,1)S(1)} %get-tuple-element.57), channel_id=1, source_target_pairs={{0,24},{1,25},{2,26},{3,27},{4,28},{5,29},{6,30},{7,31},{8,0},{9,1... | collective-permute-start | bytes 313352 | tf_op jit(solution)/shard_map/ppermute | solution.py:649
  15.0 14.8 %collective-permute-start.7 = (bf16[512,128]{1,0:T(8,128)(2,1)S(1)}, bf16[512,128]{1,0:T(8,128)(2,1)S(1)}, u32[]{:S(2)}, u32[]{:S(2)}) collective-permute-start(bf16[512,128]{1,0:T(8,128)(2,1)S(1)} %shard_map.192), channel_id=1, source_target_pairs={{0,4},{1,5},{2,6},{3,7},{4,0},{5,1},{6,2},{7,3},{8,12},{9,13},{10,... | collective-permute-start | bytes 393224 | tf_op jit(solution)/shard_map/ppermute | solution.py:649
  18.3 7.1 %collective-permute-start.3 = (bf16[136,256]{1,0:T(8,128)(2,1)S(1)}, bf16[136,256]{1,0:T(8,128)(2,1)S(1)}, u32[]{:S(2)}, u32[]{:S(2)}) collective-permute-start(bf16[136,256]{1,0:T(8,128)(2,1)S(1)} %get-tuple-element.58), channel_id=1, source_target_pairs={{0,4},{1,5},{2,6},{3,7},{4,0},{5,1},{6,2},{7,3},{8,12},{9,13},{10,... | collective-permute-start | bytes 208904 | tf_op jit(solution)/shard_map/ppermute | solution.py:649
  18.9 7.7 %collective-permute-start.4 = (bf16[136,256]{1,0:T(8,128)(2,1)S(1)}, bf16[136,256]{1,0:T(8,128)(2,1)S(1)}, u32[]{:S(2)}, u32[]{:S(2)}) collective-permute-start(bf16[136,256]{1,0:T(8,128)(2,1)S(1)} %get-tuple-element.59), channel_id=1, source_target_pairs={{0,12},{1,13},{2,14},{3,15},{4,8},{5,9},{6,10},{7,11},{8,20},{9,21... | collective-permute-start | bytes 208904 | tf_op jit(solution)/shard_map/ppermute | solution.py:649
  22.6 6.9 %collective-permute-start.5 = (bf16[136,256]{1,0:T(8,128)(2,1)S(1)}, bf16[136,256]{1,0:T(8,128)(2,1)S(1)}, u32[]{:S(2)}, u32[]{:S(2)}) collective-permute-start(bf16[136,256]{1,0:T(8,128)(2,1)S(1)} %get-tuple-element.60), channel_id=1, source_target_pairs={{0,20},{1,21},{2,22},{3,23},{4,16},{5,17},{6,18},{7,19},{8,28},{9,... | collective-permute-start | bytes 208904 | tf_op jit(solution)/shard_map/ppermute | solution.py:649
  24.1 5.7 %collective-permute-start.6 = (bf16[136,256]{1,0:T(8,128)(2,1)S(1)}, bf16[136,256]{1,0:T(8,128)(2,1)S(1)}, u32[]{:S(2)}, u32[]{:S(2)}) collective-permute-start(bf16[136,256]{1,0:T(8,128)(2,1)S(1)} %get-tuple-element.61), channel_id=1, source_target_pairs={{0,28},{1,29},{2,30},{3,31},{4,24},{5,25},{6,26},{7,27},{8,4},{9,5... | collective-permute-start | bytes 208904 | tf_op jit(solution)/shard_map/ppermute | solution.py:649
  32.0 5.0 %collective-permute-start.8 = (bf16[512,128]{1,0:T(8,128)(2,1)S(1)}, bf16[512,128]{1,0:T(8,128)(2,1)S(1)}, u32[]{:S(2)}, u32[]{:S(2)}) collective-permute-start(bf16[512,128]{1,0:T(8,128)(2,1)S(1)} %get-tuple-element.67), channel_id=1, source_target_pairs={{0,4},{1,5},{2,6},{3,7},{4,0},{5,1},{6,2},{7,3},{8,12},{9,13},{10,... | collective-permute-start | bytes 393224 | tf_op jit(solution)/shard_map/ppermute | solution.py:649
  37.1 6.3 %collective-permute-start.10 = (bf16[128,256]{1,0:T(8,128)(2,1)S(1)}, bf16[128,256]{1,0:T(8,128)(2,1)S(1)}, u32[]{:S(2)}, u32[]{:S(2)}) collective-permute-start(bf16[128,256]{1,0:T(8,128)(2,1)S(1)} %get-tuple-element.70), channel_id=1, source_target_pairs={{0,16},{1,17},{2,18},{3,19},{4,20},{5,21},{6,22},{7,23},{8,24},{9,... | collective-permute-start | bytes 196616 | tf_op jit(solution)/shard_map/ppermute | solution.py:649
  38.4 5.0 %collective-permute-start.11 = (bf16[128,256]{1,0:T(8,128)(2,1)S(1)}, bf16[128,256]{1,0:T(8,128)(2,1)S(1)}, u32[]{:S(2)}, u32[]{:S(2)}) collective-permute-start(bf16[128,256]{1,0:T(8,128)(2,1)S(1)} %get-tuple-element.71), channel_id=1, source_target_pairs={{0,24},{1,25},{2,26},{3,27},{4,28},{5,29},{6,30},{7,31},{8,0},{9,1... | collective-permute-start | bytes 196616 | tf_op jit(solution)/shard_map/ppermute | solution.py:649
  40.6 6.1 %collective-permute-start.9 = (bf16[128,256]{1,0:T(8,128)(2,1)S(1)}, bf16[128,256]{1,0:T(8,128)(2,1)S(1)}, u32[]{:S(2)}, u32[]{:S(2)}) collective-permute-start(bf16[128,256]{1,0:T(8,128)(2,1)S(1)} %get-tuple-element.69), channel_id=1, source_target_pairs={{0,8},{1,9},{2,10},{3,11},{4,12},{5,13},{6,14},{7,15},{8,16},{9,17... | collective-permute-start | bytes 196616 | tf_op jit(solution)/shard_map/ppermute | solution.py:649
  46.9 5.2 %collective-permute-start.12 = (f32[8,128]{1,0:T(8,128)S(1)}, f32[8,128]{1,0:T(8,128)S(1)}, u32[]{:S(2)}, u32[]{:S(2)}) collective-permute-start(f32[8,128]{1,0:T(8,128)S(1)} %get-tuple-element.74.refs_3_), channel_id=1, source_target_pairs={{0,1},{1,0},{2,3},{3,2},{4,5},{5,4},{6,7},{7,6},{8,9},{9,8},{10,11... | collective-permute-start | bytes 12296 | tf_op jit(solution)/shard_map/ppermute | solution.py:649
  47.0 5.1 %collective-permute-start.13 = (f32[8,128]{1,0:T(8,128)S(1)}, f32[8,128]{1,0:T(8,128)S(1)}, u32[]{:S(2)}, u32[]{:S(2)}) collective-permute-start(f32[8,128]{1,0:T(8,128)S(1)} %get-tuple-element.74.refs_3_), channel_id=1, source_target_pairs={{0,2},{1,3},{2,0},{3,1},{4,6},{5,7},{6,4},{7,5},{8,10},{9,11},{10,... | collective-permute-start | bytes 12296 | tf_op jit(solution)/shard_map/ppermute | solution.py:649
  56.1 7.4 %collective-permute-start.16 = (bf16[48,2048]{1,0:T(8,128)(2,1)S(1)}, bf16[48,2048]{1,0:T(8,128)(2,1)S(1)}, u32[]{:S(2)}, u32[]{:S(2)}) collective-permute-start(bf16[48,2048]{1,0:T(8,128)(2,1)S(1)} %get-tuple-element.80), channel_id=1, source_target_pairs={{0,2},{1,3},{2,0},{3,1},{4,6},{5,7},{6,4},{7,5},{8,10},{9,11},{10,... | collective-permute-start | bytes 589832 | tf_op jit(solution)/shard_map/ppermute | solution.py:649
  57.8 5.6 %collective-permute-start.18 = (f32[2,512]{1,0:T(2,128)S(1)}, f32[2,512]{1,0:T(2,128)S(1)}, u32[]{:S(2)}, u32[]{:S(2)}) collective-permute-start(f32[2,512]{1,0:T(2,128)S(1)} %pad_maximum_fusion.1.l0), channel_id=1, source_target_pairs={{0,2},{1,3},{2,0},{3,1},{4,6},{5,7},{6,4},{7,5},{8,10},{9,11},{10,... | collective-permute-start | bytes 12296 | tf_op jit(solution)/shard_map/ppermute | solution.py:649
  58.3 5.1 %collective-permute-start.19 = (f32[2,512]{1,0:T(2,128)S(1)}, f32[2,512]{1,0:T(2,128)S(1)}, u32[]{:S(2)}, u32[]{:S(2)}) collective-permute-start(f32[2,512]{1,0:T(2,128)S(1)} %pad_maximum_fusion.1.l0), channel_id=1, source_target_pairs={{0,3},{1,2},{2,1},{3,0},{4,7},{5,6},{6,5},{7,4},{8,11},{9,10},{10,... | collective-permute-start | bytes 12296 | tf_op jit(solution)/shard_map/ppermute | solution.py:649
  64.3 11.8 %collective-permute-start.21 = (bf16[48,2176]{1,0:T(8,128)(2,1)S(1)}, bf16[48,2176]{1,0:T(8,128)(2,1)S(1)}, u32[]{:S(2)}, u32[]{:S(2)}) collective-permute-start(bf16[48,2176]{1,0:T(8,128)(2,1)S(1)} %collective-permute-done.20.refs_0_.s0), channel_id=1, source_target_pairs={{0,4},{1,5},{2,6},{3,7},{4,0},{5,1},{6,2},{7,3},{8,12},{9,13},{10,... | collective-permute-start | bytes 626696 | tf_op jit(solution)/shard_map/ppermute | solution.py:649
  65.4 14.9 %collective-permute-start.22 = (bf16[48,2176]{1,0:T(8,128)(2,1)S(1)}, bf16[48,2176]{1,0:T(8,128)(2,1)S(1)}, u32[]{:S(2)}, u32[]{:S(2)}) collective-permute-start(bf16[48,2176]{1,0:T(8,128)(2,1)S(1)} %collective-permute-done.20.refs_0_.s0), channel_id=1, source_target_pairs={{0,2},{1,3},{2,0},{3,1},{4,6},{5,7},{6,4},{7,5},{8,10},{9,11},{10,... | collective-permute-start | bytes 626696 | tf_op jit(solution)/shard_map/ppermute | solution.py:649
  76.1 9.9 %collective-permute-start.23 = (bf16[48,2176]{1,0:T(8,128)(2,1)S(1)}, bf16[48,2176]{1,0:T(8,128)(2,1)S(1)}, u32[]{:S(2)}, u32[]{:S(2)}) collective-permute-start(bf16[48,2176]{1,0:T(8,128)(2,1)S(1)} %collective-permute-done.20.refs_0_.s0), channel_id=1, source_target_pairs={{0,1},{1,0},{2,3},{3,2},{4,5},{5,4},{6,7},{7,6},{8,9},{9,8},{10,11... | collective-permute-start | bytes 626696 | tf_op jit(solution)/shard_map/ppermute | solution.py:649
  76.1 10.0 %collective-permute-start.24 = (bf16[48,2176]{1,0:T(8,128)(2,1)S(1)}, bf16[48,2176]{1,0:T(8,128)(2,1)S(1)}, u32[]{:S(2)}, u32[]{:S(2)}) collective-permute-start(bf16[48,2176]{1,0:T(8,128)(2,1)S(1)} %collective-permute-done.21.refs_1_), channel_id=1, source_target_pairs={{0,1},{1,0},{2,3},{3,2},{4,5},{5,4},{6,7},{7,6},{8,9},{9,8},{10,11... | collective-permute-start | bytes 626696 | tf_op jit(solution)/shard_map/ppermute | solution.py:649
  80.3 5.7 %collective-permute-start.25 = (bf16[48,2176]{1,0:T(8,128)(2,1)S(1)}, bf16[48,2176]{1,0:T(8,128)(2,1)S(1)}, u32[]{:S(2)}, u32[]{:S(2)}) collective-permute-start(bf16[48,2176]{1,0:T(8,128)(2,1)S(1)} %collective-permute-done.22.refs_2_.s1), channel_id=1, source_target_pairs={{0,1},{1,0},{2,3},{3,2},{4,5},{5,4},{6,7},{7,6},{8,9},{9,8},{10,11... | collective-permute-start | bytes 626696 | tf_op jit(solution)/shard_map/ppermute | solution.py:649
  90.1 11.6 %collective-permute-start.26 = (bf16[288,1024]{1,0:T(8,128)(2,1)S(1)}, bf16[288,1024]{1,0:T(8,128)(2,1)S(1)}, u32[]{:S(2)}, u32[]{:S(2)}) collective-permute-start(bf16[288,1024]{1,0:T(8,128)(2,1)S(1)} %get-tuple-element.87), channel_id=1, source_target_pairs={{0,1},{1,0},{2,3},{3,2},{4,5},{5,4},{6,7},{7,6},{8,9},{9,8},{10,11... | collective-permute-start | bytes 1769480 | tf_op jit(solution)/shard_map/ppermute | solution.py:649
  90.7 7.2 %collective-permute-start.29 = (bf16[48,2176]{1,0:T(8,128)(2,1)S(1)}, bf16[48,2176]{1,0:T(8,128)(2,1)S(1)}, u32[]{:S(2)}, u32[]{:S(2)}) collective-permute-start(bf16[48,2176]{1,0:T(8,128)(2,1)S(1)} %collective-permute-done.21.refs_1_), channel_id=1, source_target_pairs={{0,2},{1,3},{2,0},{3,1},{4,6},{5,7},{6,4},{7,5},{8,10},{9,11},{10,... | collective-permute-start | bytes 626696 | tf_op jit(solution)/shard_map/ppermute | solution.py:649
  101.8 13.6 %collective-permute-start.27 = (bf16[192,512]{1,0:T(8,128)(2,1)S(1)}, bf16[192,512]{1,0:T(8,128)(2,1)S(1)}, u32[]{:S(2)}, u32[]{:S(2)}) collective-permute-start(bf16[192,512]{1,0:T(8,128)(2,1)S(1)} %get-tuple-element.89), channel_id=1, source_target_pairs={{0,2},{1,3},{2,0},{3,1},{4,6},{5,7},{6,4},{7,5},{8,10},{9,11},{10,... | collective-permute-start | bytes 589832 | tf_op jit(solution)/shard_map/ppermute | solution.py:649
  103.7 5.6 %collective-permute-start.32 = (bf16[96,512]{1,0:T(8,128)(2,1)S(1)}, bf16[96,512]{1,0:T(8,128)(2,1)S(1)}, u32[]{:S(2)}, u32[]{:S(2)}) collective-permute-start(bf16[96,512]{1,0:T(8,128)(2,1)S(1)} %get-tuple-element.94), channel_id=1, source_target_pairs={{0,4},{1,5},{2,6},{3,7},{4,0},{5,1},{6,2},{7,3},{8,12},{9,13},{10,... | collective-permute-start | bytes 294920 | tf_op jit(solution)/shard_map/ppermute | solution.py:649
  104.8 7.3 %collective-permute-start.33 = (bf16[96,512]{1,0:T(8,128)(2,1)S(1)}, bf16[96,512]{1,0:T(8,128)(2,1)S(1)}, u32[]{:S(2)}, u32[]{:S(2)}) collective-permute-start(bf16[96,512]{1,0:T(8,128)(2,1)S(1)} %get-tuple-element.95), channel_id=1, source_target_pairs={{0,6},{1,7},{2,4},{3,5},{4,2},{5,3},{6,0},{7,1},{8,14},{9,15},{10,... | collective-permute-start | bytes 294920 | tf_op jit(solution)/shard_map/ppermute | solution.py:649
  106.3 7.2 %collective-permute-start.28 = (bf16[96,512]{1,0:T(8,128)(2,1)S(1)}, bf16[96,512]{1,0:T(8,128)(2,1)S(1)}, u32[]{:S(2)}, u32[]{:S(2)}) collective-permute-start(bf16[96,512]{1,0:T(8,128)(2,1)S(1)} %get-tuple-element.90), channel_id=1, source_target_pairs={{0,4},{1,5},{2,6},{3,7},{4,0},{5,1},{6,2},{7,3},{8,12},{9,13},{10,... | collective-permute-start | bytes 294920 | tf_op jit(solution)/shard_map/ppermute | solution.py:649
  107.3 8.1 %collective-permute-start.34 = (bf16[96,512]{1,0:T(8,128)(2,1)S(1)}, bf16[96,512]{1,0:T(8,128)(2,1)S(1)}, u32[]{:S(2)}, u32[]{:S(2)}) collective-permute-start(bf16[96,512]{1,0:T(8,128)(2,1)S(1)} %get-tuple-element.96), channel_id=1, source_target_pairs={{0,6},{1,7},{2,4},{3,5},{4,2},{5,3},{6,0},{7,1},{8,14},{9,15},{10,... | collective-permute-start | bytes 294920 | tf_op jit(solution)/shard_map/ppermute | solution.py:649
  120.0 6.5 %collective-permute-start.38 = (bf16[48,512]{1,0:T(8,128)(2,1)S(1)}, bf16[48,512]{1,0:T(8,128)(2,1)S(1)}, u32[]{:S(2)}, u32[]{:S(2)}) collective-permute-start(bf16[48,512]{1,0:T(8,128)(2,1)S(1)} %get-tuple-element.100), channel_id=1, source_target_pairs={{0,8},{1,9},{2,10},{3,11},{4,12},{5,13},{6,14},{7,15},{8,16},{9,17... | collective-permute-start | bytes 147464 | tf_op jit(solution)/shard_map/ppermute | solution.py:649
  120.1 7.6 %collective-permute-start.39 = (bf16[48,512]{1,0:T(8,128)(2,1)S(1)}, bf16[48,512]{1,0:T(8,128)(2,1)S(1)}, u32[]{:S(2)}, u32[]{:S(2)}) collective-permute-start(bf16[48,512]{1,0:T(8,128)(2,1)S(1)} %get-tuple-element.101), channel_id=1, source_target_pairs={{0,16},{1,17},{2,18},{3,19},{4,20},{5,21},{6,22},{7,23},{8,24},{9,... | collective-permute-start | bytes 147464 | tf_op jit(solution)/shard_map/ppermute | solution.py:649
  121.1 6.6 %collective-permute-start.40 = (bf16[48,512]{1,0:T(8,128)(2,1)S(1)}, bf16[48,512]{1,0:T(8,128)(2,1)S(1)}, u32[]{:S(2)}, u32[]{:S(2)}) collective-permute-start(bf16[48,512]{1,0:T(8,128)(2,1)S(1)} %get-tuple-element.102), channel_id=1, source_target_pairs={{0,24},{1,25},{2,26},{3,27},{4,28},{5,29},{6,30},{7,31},{8,0},{9,1... | collective-permute-start | bytes 147464 | tf_op jit(solution)/shard_map/ppermute | solution.py:649
  (15 other events, 178.1 us)
